TPU v7x, 32 devices: a whole 2x2x4 slice. The times are simulated.
32 devices in a mesh: ep: 8 (over z, x), tp: 4 (over y, core).
Axes of the slice: x: 2, y: 2, z: 4, core: 2. Of those that a mesh axis runs over, the one named last changes fastest.
Arguments:
- queries: bfloat16 [1024, 512], P('ep'), may hold values from -6 to 6
- key_vectors: bfloat16 [1024, 512], P('ep'), may hold values from -6 to 6
- values: bfloat16 [1024, 1024], P('ep', 'tp'), may hold values from -6 to 6
- out_gate: bfloat16 [1024, 1024], P('ep', 'tp'), may hold values from -6 to 6
- input_gate: float32 [1024, 2], P('ep'), may hold values from -8 to 130
- forget_gate: float32 [1024, 2], P('ep'), may hold values from -2 to 16
- mix_weight: bfloat16 [1024, 2048], P('tp'), may hold values from -0.1875 to 0.1875
- expert_input: bfloat16 [2048, 2048], P('ep'), may hold values from -6 to 6
- norm_gain: float32 [2048], replicated, may hold values from 0.1 to 1.9
- route_ids: int32 [2048, 4], P('ep'), may hold values from 0 to 7, all different within a row; in each aligned block of 256 rows (0 to 255, 256 to 511, ...) at most 256 rows name the same one
- route_weights: float32 [2048, 4], P('ep'), may hold values from 0.2 to 1.2
- expert_gate: bfloat16 [32, 2048, 256], P(('ep', 'tp')), may hold values from -0.125 to 0.125
- expert_up: bfloat16 [32, 2048, 256], P(('ep', 'tp')), may hold values from -0.125 to 0.125
- expert_down: bfloat16 [32, 256, 2048], P(('ep', 'tp')), may hold values from -0.1875 to 0.1875
- shared_gate: bfloat16 [2048, 512], P(None, 'tp'), may hold values from -0.125 to 0.125
- shared_up: bfloat16 [2048, 512], P(None, 'tp'), may hold values from -0.125 to 0.125
- shared_down: bfloat16 [512, 2048], P('tp'), may hold values from -0.25 to 0.25
Outputs:
- mixer_out: bfloat16 [1024, 2048], P('ep')
- expert_out: bfloat16 [2048, 2048], P('ep')
Inputs may be any that keep to these rules, and one draw needn't show every extreme that they name: `route_ids`: each row names 4 different experts. In each aligned block of 256 rows (the rows of one index of ep) no expert is named by more than 256 rows, and in some block one expert is named by exactly 256 rows.
All inputs are finite; a program needn't handle non-finite values.
Results may differ from a plain program's by a relative error of at most 0.01575.
Values may be sent and summed in bfloat16 or wider, within the bound.
A program may use at most 64 MiB of HBM per device.

v0:
```python
import functools

import jax
import jax.numpy as jnp
from jax import lax
from jax.experimental import pallas as pl
from jax.experimental.pallas import tpu as pltpu
from jax.sharding import PartitionSpec as P

D = 2048
MEMORY_HEADS = 2
KEY_DIM = 256
BLOCK = 128
FF = 1024


epsilon = 1e-06
lowest = -1e30
den_floor = 4.0


def mixer_local(queries, key_vectors, values, input_gate, forget_gate):
    tp_count = lax.axis_size("tp")
    tp_rank = lax.axis_index("tp")
    head_index = tp_rank // (tp_count // MEMORY_HEADS)
    offset = head_index * KEY_DIM
    query_head = lax.dynamic_slice_in_dim(queries, offset, KEY_DIM, 1)
    key_head = lax.dynamic_slice_in_dim(key_vectors, offset, KEY_DIM, 1)
    select = jnp.arange(MEMORY_HEADS, dtype=jnp.int32)[None, :] == head_index
    gates = jnp.stack(
        [
            jnp.sum(jnp.where(select, input_gate, 0.0), axis=1),
            jax.nn.log_sigmoid(jnp.sum(jnp.where(select, forget_gate, 0.0), axis=1)),
        ]
    )
    return query_head, jnp.concatenate([key_head, values], axis=1), gates


def mixer_rows(query_head, both, gates, out_gate):
    ep_count = lax.axis_size("ep")
    ep_rank = lax.axis_index("ep")
    length = query_head.shape[0]
    factor = KEY_DIM ** (-0.5)
    keys_all = both[:, :KEY_DIM]
    values_all = both[:, KEY_DIM:]
    total = ep_count * length
    blocks = total // BLOCK
    mine = length // BLOCK
    input_all = gates[0].reshape(blocks, BLOCK)
    cumulative = jnp.cumsum(gates[1].reshape(blocks, BLOCK), axis=1)
    block_total = cumulative[:, -1]
    index = jnp.arange(blocks, dtype=jnp.int32)
    here = ep_rank * mine + jnp.arange(mine, dtype=jnp.int32)
    between = (index[None, None, :] > index[None, :, None]) & (
        index[None, None, :] < here[:, None, None]
    )
    gap = jnp.sum(jnp.where(between, block_total[None, None, :], 0.0), axis=2)
    ahead = jnp.sum(jnp.where(index[None, :] < here[:, None], block_total[None, :], 0.0), axis=1)
    keep = block_total[:, None] - cumulative + input_all
    own_cumulative = lax.dynamic_slice_in_dim(cumulative, ep_rank * mine, mine, 0)
    same = index[None, :] == here[:, None]
    column = jnp.where(same[:, :, None], input_all - cumulative, keep + gap[:, :, None])
    log_weight = own_cumulative[:, :, None, None] + column[:, None]
    row_at = jnp.arange(BLOCK, dtype=jnp.int32)
    visible = (index[None, :] < here[:, None])[:, None, :, None] | (
        same[:, None, :, None] & (row_at[None, :, None, None] >= row_at[None, None, None, :])
    )
    log_weight = jnp.where(visible, log_weight, -jnp.inf).reshape(length, total)
    carried = (own_cumulative + ahead[:, None]).reshape(length)
    stabilizer = jnp.maximum(carried, jnp.max(log_weight, axis=1))
    within = jnp.exp(log_weight - stabilizer[:, None])
    scores = (
        jnp.einsum("td,sd->ts", query_head, keys_all, preferred_element_type=jnp.float32) * factor
    )
    weights = scores * within
    numerator = jnp.dot(
        weights.astype(jnp.bfloat16), values_all, preferred_element_type=jnp.float32
    )
    denominator = jnp.sum(weights, axis=1)
    hidden = numerator / jnp.maximum(jnp.abs(denominator), den_floor)[:, None]
    gated_rows = (hidden * jax.nn.sigmoid(out_gate.astype(jnp.float32))).astype(jnp.bfloat16)
    return gated_rows


def dense_kernel(
    lines, teams, x_ref, side_ref, kv_ref, sact_ref, g_ref, u_ref, d_ref, sd_ref, mw_ref,
    eo_ref, kvo_ref, so_ref, mwo_ref,
    tok, act, dq, sdq, mwq, sall, kvb, sideb, xout, xin, own, zout, zin, fin,
    z_send, z_recv, x_send, x_recv, c_send, c_recv, a_send, a_recv,
    k_send, k_recv, kx_send, kx_recv, w_send, w_recv, xo_send, xo_recv, zo_send, zo_recv, f_send, f_recv,
):
    me = lax.axis_index("ep")
    j = lax.axis_index("tp")
    z, x = me // 2, me % 2
    tokens = x_ref.shape[0]
    half_rows = tokens // 2
    core = j % 2
    buddy = j + 1 - 2 * core
    quarter = fin.shape[2]
    mine_rows = pl.ds(pl.multiple_of(core * half_rows, half_rows), half_rows)
    other_rows = pl.ds(pl.multiple_of((1 - core) * half_rows, half_rows), half_rows)

    def remote(src, dst, send, recv, ep, tp):
        return pltpu.make_async_remote_copy(
            src_ref=src, dst_ref=dst, send_sem=send, recv_sem=recv,
            device_id={"ep": ep, "tp": tp}, device_id_type=pl.DeviceIdType.MESH,
        )

    barrier = pltpu.get_barrier_semaphore()

    def greet(ep, tp):
        pl.semaphore_signal(
            barrier, inc=1, device_id={"ep": ep, "tp": tp}, device_id_type=pl.DeviceIdType.MESH
        )

    greet(z * 2 + 1 - x, j)
    for k in range(1, lines):
        greet(lax.rem(z + k, lines) * 2 + x, j)
    for k in range(1, teams):
        greet(me, lax.rem(j + k, teams))
    pl.semaphore_wait(barrier, lines + teams - 1)

    def columns(ref, q):
        return ref.at[:, pl.ds(pl.multiple_of(q * quarter, quarter), quarter)]

    def team_copies(k):
        p = lax.rem(j + k, teams)
        pairs = (
            (sact_ref, sall.at[j]),
            (columns(sd_ref, p), sdq.at[j]),
            (columns(mw_ref, p), mwq.at[j]),
            (columns(d_ref, p), dq.at[j]),
        )
        return [
            remote(src, dst, w_send.at[n, k - 1], w_recv.at[n, k - 1], me, p)
            for n, (src, dst) in enumerate(pairs)
        ]

    def z_copy(zb, way):
        to = z + 1 - 2 * way
        ref = tok.at[zb * 2 + x, mine_rows]
        return remote(ref, ref, z_send.at[way, zb], z_recv.at[zb], to * 2 + x, j)

    def x_copy(zb):
        ref = tok.at[zb * 2 + x, mine_rows]
        return remote(ref, ref, x_send.at[zb], x_recv.at[zb], z * 2 + 1 - x, j)

    def x_arrival(zb):
        ref = tok.at[zb * 2 + 1 - x, mine_rows]
        return remote(ref, ref, x_send.at[zb], x_recv.at[zb], z * 2 + 1 - x, j)

    def c_copy(block):
        ref = tok.at[block, mine_rows]
        return remote(ref, ref, c_send.at[block], c_recv.at[block], me, buddy)

    def c_arrival(block):
        ref = tok.at[block, other_rows]
        return remote(ref, ref, c_send.at[block], c_recv.at[block], me, buddy)

    def a_copy(block, k):
        p = lax.rem(j + k, teams)
        return remote(
            act.at[block, j], act.at[block, j],
            a_send.at[block, k - 1], a_recv.at[block, k - 1], me, p,
        )

    extras = (sideb, kvb)

    def k_copy(n, zb, way):
        to = z + 1 - 2 * way
        ref = extras[n].at[zb * 2 + x]
        return remote(ref, ref, k_send.at[n, way, zb], k_recv.at[n, zb], to * 2 + x, j)

    def kx_copy(n, zb):
        ref = extras[n].at[zb * 2 + x]
        return remote(ref, ref, kx_send.at[n, zb], kx_recv.at[n, zb], z * 2 + 1 - x, j)

    def kx_arrival(n, zb):
        ref = extras[n].at[zb * 2 + 1 - x]
        return remote(ref, ref, kx_send.at[n, zb], kx_recv.at[n, zb], z * 2 + 1 - x, j)

    tok[me] = x_ref[...]
    sideb[me] = side_ref[...]
    kvb[me] = kv_ref[...]
    for way in range(2):
        to = z + 1 - 2 * way

        @pl.when((to >= 0) & (to < lines))
        def _():
            remote(
                x_ref.at[mine_rows], tok.at[me, mine_rows],
                z_send.at[way, z], z_recv.at[z], to * 2 + x, j,
            ).start()
            for n, ref in enumerate((side_ref, kv_ref)):
                remote(
                    ref, extras[n].at[me], k_send.at[n, way, z], k_recv.at[n, z], to * 2 + x, j
                ).start()

    remote(
        x_ref.at[mine_rows], tok.at[me, mine_rows], x_send.at[z], x_recv.at[z], z * 2 + 1 - x, j
    ).start()
    for n, ref in enumerate((side_ref, kv_ref)):
        remote(
            ref, extras[n].at[me], kx_send.at[n, z], kx_recv.at[n, z], z * 2 + 1 - x, j
        ).start()
    for k in range(1, teams):
        for copy in team_copies(k):
            copy.start()
    sall[j] = sact_ref[...]
    sdq[j] = columns(sd_ref, j)[...]
    mwq[j] = columns(mw_ref, j)[...]
    dq[j] = columns(d_ref, j)[...]

    def forward(zb, d):
        z_copy(zb, d).wait_recv()
        to = z + 1 - 2 * d

        @pl.when((to >= 0) & (to < lines))
        def _():
            z_copy(zb, d).start()

        x_copy(zb).start()
        c_copy(zb * 2 + x).start()
        for n in range(2):
            k_copy(n, zb, d).wait_recv()

            @pl.when((to >= 0) & (to < lines))
            def _():
                k_copy(n, zb, d).start()

            kx_copy(n, zb).start()

    def activate(block):
        rows = tok[block]
        gate = jnp.dot(rows, g_ref[...], preferred_element_type=jnp.float32)
        up = jnp.dot(rows, u_ref[...], preferred_element_type=jnp.float32)
        act[block, j] = (gate / (1.0 + jnp.exp(-gate)) * up).astype(jnp.bfloat16)
        for e in range(1, teams // 2):
            a_move(block, j, e - 1, lax.rem(j + 2 * e, teams)).start()
        a_move(block, j, teams // 2 - 1, buddy).start()

    def a_move(block, source, slot, to):
        ref = act.at[block, source]
        return remote(ref, ref, a_send.at[block, slot], a_recv.at[block, slot], me, to)

    def finish(block):
        for e in range(1, teams // 2):
            source = lax.rem(j + teams - 2 * e, teams)
            a_move(block, source, e - 1, source).wait_recv()
            a_move(block, source, teams // 2 - 1 + e, buddy).start()
        for e in range(teams // 2):
            source = lax.rem(buddy + teams - 2 * e, teams)
            a_move(block, source, teams // 2 - 1 + e, buddy).wait_recv()
        total = jnp.dot(act[block, 0], dq[0], preferred_element_type=jnp.float32)
        for q in range(1, teams):
            total += jnp.dot(act[block, q], dq[q], preferred_element_type=jnp.float32)
        weight = sideb[block, pl.ds(me, 1), :tokens]
        row = lax.broadcasted_iota(jnp.int32, (tokens, tokens), 0)
        lane = lax.broadcasted_iota(jnp.int32, (tokens, tokens), 1)
        weight = jnp.sum(jnp.where(row == lane, weight, 0.0), axis=1, keepdims=True)
        return (total * weight).astype(jnp.bfloat16)

    def xo_copy(zb):
        return remote(
            xout.at[zb], xin.at[zb], xo_send.at[zb], xo_recv.at[zb], z * 2 + 1 - x, j
        )

    def zo_copy(zb):
        return remote(
            zout.at[zb], zin.at[z], zo_send.at[zb], zo_recv.at[z], zb * 2 + x, j
        )

    def zo_arrival(zb):
        return remote(
            zout.at[zb], zin.at[zb], zo_send.at[zb], zo_recv.at[zb], zb * 2 + x, j
        )

    def valid(s, d, zb):
        return (s >= 0) & (s < lines) & (zb >= 0) & (zb < lines) & ((s > 0) | (d == 0))

    def step(t, carry):
        def stage_one(d, carry):
            s = t
            zb = z + s * (2 * d - 1)

            @pl.when(valid(s, d, zb) & (s > 0))
            def _():
                forward(zb, d)

            return carry

        lax.fori_loop(0, 2, stage_one, 0)

        def stage_two(d, carry):
            s = t - 1
            zb = z + s * (2 * d - 1)

            @pl.when(valid(s, d, zb))
            def _():
                x_arrival(zb).wait_recv()
                c_copy(zb * 2 + 1 - x).start()
                for n in range(2):
                    kx_arrival(n, zb).wait_recv()

                def column(n, carry):
                    block = zb * 2 + lax.rem(x + n, 2)

                    @pl.when(block != me)
                    def _():
                        c_arrival(block).wait_recv()

                    activate(block)
                    return carry

                lax.fori_loop(0, 2, column, 0)

            return carry

        lax.fori_loop(0, 2, stage_two, 0)

        @pl.when(t == 2)
        def _():
            for k in range(1, teams):
                for copy in team_copies(k):
                    copy.wait_recv()

        def stage_three(d, carry):
            s = t - 2
            zb = z + s * (2 * d - 1)

            @pl.when(valid(s, d, zb))
            def _():
                xout[zb] = finish(zb * 2 + 1 - x)
                xo_copy(zb).start()
                own[zb] = finish(zb * 2 + x)

            return carry

        lax.fori_loop(0, 2, stage_three, 0)

        def stage_four(d, carry):
            s = t - 3
            zb = z + s * (2 * d - 1)

            @pl.when(valid(s, d, zb))
            def _():
                xo_copy(zb).wait_recv()

                @pl.when(s > 0)
                def _():
                    zout[zb] = (
                        own[zb].astype(jnp.float32) + xin[zb].astype(jnp.float32)
                    ).astype(jnp.bfloat16)
                    zo_copy(zb).start()

            return carry

        lax.fori_loop(0, 2, stage_four, 0)
        return carry

    lax.fori_loop(1, lines + 3, step, 0)

    def f_copies(k, source, rows):
        p = lax.rem(j + k, teams)
        return remote(
            rows.at[source], rows.at[source],
            f_send.at[k - 1], f_recv.at[k - 1],
            me, p,
        )

    total = own[z].astype(jnp.float32) + xin[z].astype(jnp.float32)
    for q in range(teams):
        total += jnp.dot(sall[q], sdq[q], preferred_element_type=jnp.float32)
    for k in range(1, lines):
        source = lax.rem(z + k, lines)
        zo_arrival(source).wait_recv()
        total += zin[source].astype(jnp.float32)
    fin[j] = total.astype(jnp.bfloat16)
    for k in range(1, teams):
        f_copies(k, j, fin).start()
    kvo_ref[...] = kvb[...]
    so_ref[...] = sideb[...]
    mwo_ref[...] = mwq[...]
    for k in range(1, teams):
        f_copies(k, lax.rem(j + teams - k, teams), fin).wait_recv()
    for q in range(teams):
        eo_ref[:, q * quarter : (q + 1) * quarter] = fin[q]

    for k in range(1, teams):
        f_copies(k, j, fin).wait_send()
        for copy in team_copies(k):
            copy.wait_send()

    def drain(zb, carry):
        for way in range(2):
            to = z + 1 - 2 * way
            passing = (zb <= z) if way == 0 else (zb >= z)

            @pl.when((to >= 0) & (to < lines) & passing)
            def _():
                z_copy(zb, way).wait_send()
                for n in range(2):
                    k_copy(n, zb, way).wait_send()

        x_copy(zb).wait_send()
        for n in range(2):
            kx_copy(n, zb).wait_send()
        xo_copy(zb).wait_send()

        @pl.when(zb != z)
        def _():
            zo_copy(zb).wait_send()

        def column(n, carry):
            block = zb * 2 + n

            @pl.when(block != me)
            def _():
                c_copy(block).wait_send()

            for k in range(1, teams):
                a_copy(block, k).wait_send()
            return carry

        lax.fori_loop(0, 2, column, 0)
        return carry

    lax.fori_loop(0, lines, drain, 0)


def project_kernel(teams, gated_ref, mwq_ref, mo_ref, gall, mfin, g_send, g_recv, f_send, f_recv):
    me = lax.axis_index("ep")
    j = lax.axis_index("tp")
    quarter = mfin.shape[2]

    def copy(ref, source, send, recv, k):
        return pltpu.make_async_remote_copy(
            src_ref=ref, dst_ref=source, send_sem=send.at[k - 1], recv_sem=recv.at[k - 1],
            device_id={"ep": me, "tp": lax.rem(j + k, teams)},
            device_id_type=pl.DeviceIdType.MESH,
        )

    barrier = pltpu.get_barrier_semaphore()
    for k in range(1, teams):
        pl.semaphore_signal(
            barrier, inc=1, device_id={"ep": me, "tp": lax.rem(j + k, teams)},
            device_id_type=pl.DeviceIdType.MESH,
        )
    pl.semaphore_wait(barrier, teams - 1)
    for k in range(1, teams):
        copy(gated_ref, gall.at[j], g_send, g_recv, k).start()
    gall[j] = gated_ref[...]
    for k in range(1, teams):
        source = lax.rem(j + teams - k, teams)
        copy(gated_ref, gall.at[source], g_send, g_recv, k).wait_recv()
    mixed = jnp.zeros(mfin.shape[1:], jnp.float32)
    for q in range(teams):
        mixed += (
            jnp.dot(gall[q], mwq_ref[q], preferred_element_type=jnp.float32)
            .astype(jnp.bfloat16)
            .astype(jnp.float32)
        )
    mfin[j] = mixed.astype(jnp.bfloat16)
    for k in range(1, teams):
        copy(mfin.at[j], mfin.at[j], f_send, f_recv, k).start()
    for k in range(1, teams):
        source = lax.rem(j + teams - k, teams)
        copy(mfin.at[source], mfin.at[source], f_send, f_recv, k).wait_recv()
    for q in range(teams):
        mo_ref[:, q * quarter : (q + 1) * quarter] = mfin[q]
    for k in range(1, teams):
        copy(gated_ref, gall.at[j], g_send, g_recv, k).wait_send()
        copy(mfin.at[j], mfin.at[j], f_send, f_recv, k).wait_send()


def dense_experts(
    query_head,
    both,
    gates,
    out_gate,
    mix_weight,
    expert_input,
    norm_gain,
    route_ids,
    route_weights,
    expert_gate,
    expert_up,
    expert_down,
    shared_gate,
    shared_up,
    shared_down,
):
    ep_count = lax.axis_size("ep")
    teams = lax.axis_size("tp")
    lines = ep_count // 2
    tokens, width = expert_input.shape
    quarter = width // teams
    units = expert_gate.shape[2]
    shared_units = shared_gate.shape[1]
    length, channels = both.shape[0], mix_weight.shape[0]
    rows_wide = expert_input.astype(jnp.float32)
    normed = (
        rows_wide
        * lax.rsqrt(jnp.mean(rows_wide * rows_wide, axis=-1, keepdims=True) + epsilon)
        * norm_gain
    ).astype(jnp.bfloat16)
    named = route_ids[:, :, None] == jnp.arange(ep_count, dtype=jnp.int32)[None, None, :]
    table = jnp.sum(jnp.where(named, route_weights[:, :, None], 0.0), axis=1).T
    lanes = max(tokens, length)
    side = jnp.concatenate(
        [
            jnp.pad(table, ((0, 0), (0, lanes - tokens))),
            jnp.pad(gates, ((0, -(ep_count + 2) % 8), (0, lanes - length))),
        ]
    )
    shared_gate_val = jnp.dot(normed, shared_gate, preferred_element_type=jnp.float32)
    shared_up_val = jnp.dot(normed, shared_up, preferred_element_type=jnp.float32)
    shared_act = (jax.nn.silu(shared_gate_val) * shared_up_val).astype(jnp.bfloat16)
    low, dma = jnp.bfloat16, pltpu.SemaphoreType.DMA
    vmem = pl.BlockSpec(memory_space=pltpu.VMEM)
    expert_out, both_all, side_all, mix_all = pl.pallas_call(
        functools.partial(dense_kernel, lines, teams),
        out_shape=(
            jax.ShapeDtypeStruct((tokens, width), low),
            jax.ShapeDtypeStruct((ep_count, *both.shape), low),
            jax.ShapeDtypeStruct((ep_count, *side.shape), jnp.float32),
            jax.ShapeDtypeStruct((teams, channels, quarter), low),
        ),
        in_specs=[vmem] * 9,
        out_specs=(vmem, vmem, vmem, vmem),
        scratch_shapes=[
            pltpu.VMEM((ep_count, tokens, width), low),
            pltpu.VMEM((ep_count, teams, tokens, units), low),
            pltpu.VMEM((teams, units, quarter), low),
            pltpu.VMEM((teams, shared_units, quarter), low),
            pltpu.VMEM((teams, channels, quarter), low),
            pltpu.VMEM((teams, tokens, shared_units), low),
            pltpu.VMEM((ep_count, *both.shape), low),
            pltpu.VMEM((ep_count, *side.shape), jnp.float32),
            pltpu.VMEM((lines, tokens, quarter), low),
            pltpu.VMEM((lines, tokens, quarter), low),
            pltpu.VMEM((lines, tokens, quarter), low),
            pltpu.VMEM((lines, tokens, quarter), low),
            pltpu.VMEM((lines, tokens, quarter), low),
            pltpu.VMEM((teams, tokens, quarter), low),
            dma((2, lines)), dma((lines,)), dma((lines,)), dma((lines,)),
            dma((ep_count,)), dma((ep_count,)),
            dma((ep_count, teams - 1)), dma((ep_count, teams - 1)),
            dma((2, 2, lines)), dma((2, lines)), dma((2, lines)), dma((2, lines)),
            dma((4, teams - 1)), dma((4, teams - 1)),
            dma((lines,)), dma((lines,)), dma((lines,)), dma((lines,)),
            dma((teams - 1,)), dma((teams - 1,)),
        ],
        compiler_params=pltpu.CompilerParams(
            collective_id=0, has_side_effects=True, vmem_limit_bytes=56 * 1024 * 1024
        ),
    )(
        normed, side, both, shared_act,
        expert_gate[0], expert_up[0], expert_down[0], shared_down, mix_weight,
    )
    gates_all = side_all[:, ep_count : ep_count + 2, :length].transpose(1, 0, 2)
    gated_rows = mixer_rows(
        query_head,
        both_all.reshape(ep_count * length, both.shape[1]),
        gates_all.reshape(2, ep_count * length),
        out_gate,
    )
    mixer_out = pl.pallas_call(
        functools.partial(project_kernel, teams),
        out_shape=jax.ShapeDtypeStruct((length, width), low),
        in_specs=[vmem] * 2,
        out_specs=vmem,
        scratch_shapes=[
            pltpu.VMEM((teams, length, channels), low),
            pltpu.VMEM((teams, length, quarter), low),
            dma((teams - 1,)), dma((teams - 1,)), dma((teams - 1,)), dma((teams - 1,)),
        ],
        compiler_params=pltpu.CompilerParams(collective_id=1, has_side_effects=True),
    )(gated_rows, mix_all)
    return mixer_out, expert_out


def expert_half(
    expert_input,
    norm_gain,
    route_ids,
    route_weights,
    expert_gate,
    expert_up,
    expert_down,
    shared_gate,
    shared_up,
    shared_down,
):
    ep_count = lax.axis_size("ep")
    tp_count = lax.axis_size("tp")
    tp_rank = lax.axis_index("tp")
    tokens = expert_input.shape[0]
    top_count = route_ids.shape[1]
    slice_units = expert_gate.shape[2]
    group_size = FF // slice_units
    per_ep = tp_count // group_size
    team_index = tp_rank // group_size
    expert_count = ep_count * per_ep
    capacity = 2 * tokens * top_count // expert_count
    rows_wide = expert_input.astype(jnp.float32)
    normed = (
        rows_wide
        * lax.rsqrt(jnp.mean(rows_wide * rows_wide, axis=-1, keepdims=True) + epsilon)
        * norm_gain
    ).astype(jnp.bfloat16)
    chosen = route_ids.reshape(-1)
    onehot = (chosen[:, None] == jnp.arange(expert_count, dtype=jnp.int32)[None, :]).astype(
        jnp.int32
    )
    slot_rank = jnp.sum((jnp.cumsum(onehot, axis=0) - onehot) * onehot, axis=1)
    in_team = chosen % per_ep == team_index
    target = jnp.where(in_team, chosen // per_ep * capacity + slot_rank, ep_count * capacity)
    token_of = jnp.arange(chosen.shape[0], dtype=jnp.int32) // top_count
    slot_token = jnp.zeros((ep_count * capacity,), jnp.int32).at[target].set(token_of, mode="drop")
    slot_live = jnp.zeros((ep_count * capacity,), jnp.int32).at[target].set(1, mode="drop")
    outgoing = jnp.where(slot_live[:, None] > 0, normed[slot_token], jnp.zeros((), jnp.bfloat16))
    outgoing = outgoing.reshape(ep_count, capacity, D)
    gate_slice = expert_gate[0]
    up_slice = expert_up[0]
    down_slice = expert_down[0]
    arrived = lax.all_to_all(outgoing, "ep", split_axis=0, concat_axis=0, tiled=True)
    gate_val = jnp.einsum("sid,df->sif", arrived, gate_slice, preferred_element_type=jnp.float32)
    up_val = jnp.einsum("sid,df->sif", arrived, up_slice, preferred_element_type=jnp.float32)
    hidden = (jax.nn.silu(gate_val) * up_val).astype(jnp.bfloat16)
    partial_value = jnp.einsum(
        "sif,fd->sid", hidden, down_slice, preferred_element_type=jnp.float32
    )
    partial_value = partial_value.astype(jnp.bfloat16)
    returned = lax.all_to_all(partial_value, "ep", split_axis=0, concat_axis=0, tiled=True)
    flat_back = returned.reshape(ep_count * capacity, returned.shape[2])
    gather_at = jnp.where(in_team, target, 0).reshape(tokens, top_count)
    weight_at = jnp.where(in_team, route_weights.reshape(-1), 0.0).reshape(tokens, top_count)
    combined = jnp.zeros((tokens, returned.shape[2]), jnp.float32)
    for pick_index in range(top_count):
        combined = (
            combined
            + flat_back[gather_at[:, pick_index]].astype(jnp.float32)
            * weight_at[:, pick_index][:, None]
        )
    shared_gate_val = jnp.dot(normed, shared_gate, preferred_element_type=jnp.float32)
    shared_up_val = jnp.dot(normed, shared_up, preferred_element_type=jnp.float32)
    shared_act = (jax.nn.silu(shared_gate_val) * shared_up_val).astype(jnp.bfloat16)
    return combined + jnp.dot(shared_act, shared_down, preferred_element_type=jnp.float32)


def shards(
    queries,
    key_vectors,
    values,
    out_gate,
    input_gate,
    forget_gate,
    mix_weight,
    expert_input,
    norm_gain,
    route_ids,
    route_weights,
    expert_gate,
    expert_up,
    expert_down,
    shared_gate,
    shared_up,
    shared_down,
):
    ep_count, tp_count = lax.axis_size("ep"), lax.axis_size("tp")
    tokens, slots = expert_input.shape[0], route_ids.shape[1] * 2 * expert_input.shape[0]
    per_ep = tp_count * expert_gate.shape[2] // FF
    even = ep_count % 2 == 0 and tp_count % 2 == 0
    dense = even and per_ep == 1 and slots // (ep_count * per_ep) >= tokens
    query_head, both, gates = mixer_local(
        queries, key_vectors, values, input_gate, forget_gate
    )
    experts = (
        expert_input,
        norm_gain,
        route_ids,
        route_weights,
        expert_gate,
        expert_up,
        expert_down,
        shared_gate,
        shared_up,
        shared_down,
    )
    if dense:
        return dense_experts(query_head, both, gates, out_gate, mix_weight, *experts)
    both = lax.all_gather(both, "ep", axis=0, tiled=True)
    gates = lax.all_gather(gates, "ep", axis=1, tiled=True)
    gated_rows = mixer_rows(query_head, both, gates, out_gate)
    mixer_partial = jnp.dot(gated_rows, mix_weight, preferred_element_type=jnp.float32)
    expert_partial = expert_half(*experts)
    mixer_piece = lax.psum_scatter(
        mixer_partial.astype(jnp.bfloat16), "tp", scatter_dimension=0, tiled=True
    )
    mixer_out = lax.all_gather(mixer_piece, "tp", axis=0, tiled=True)
    expert_piece = lax.psum_scatter(expert_partial, "tp", scatter_dimension=0, tiled=True).astype(
        jnp.bfloat16
    )
    expert_out = lax.all_gather(expert_piece, "tp", axis=0, tiled=True)
    return (mixer_out, expert_out)


def solution(mesh):
    return jax.shard_map(
        shards,
        mesh=mesh,
        in_specs=(
            P("ep", None),
            P("ep", None),
            P("ep", "tp"),
            P("ep", "tp"),
            P("ep", None),
            P("ep", None),
            P("tp", None),
            P("ep", None),
            P(),
            P("ep", None),
            P("ep", None),
            P(("ep", "tp"), None, None),
            P(("ep", "tp"), None, None),
            P(("ep", "tp"), None, None),
            P(None, "tp"),
            P(None, "tp"),
            P("tp", None),
        ),
        out_specs=(P("ep", None), P("ep", None)),
        check_vma=False,
    )
```

profile of v0, /device:TPU:25, one launch (start us, length us, event | category | flops | bytes accessed | tf_op | source)
XLA Modules:
  0.0 157.6 jit_solution(13238885284118356484)
XLA Ops:
  0.6 0.0 copy-start
  0.6 0.0 copy-start.2
  0.7 1.0 constant_dynamic-slice_fusion.1
  1.6 1.5 pad_maximum_fusion.kv_ref
  3.2 0.8 select_reduce_fusion.4
  4.0 0.7 select_reduce_fusion.1
  4.7 0.6 pad_maximum_fusion.1.side_ref
  5.3 1.5 fusion
  6.8 0.3 fusion.2.x_ref
  7.1 0.0 copy-start.1
  7.2 0.0 copy-start.6
  7.2 0.4 fusion.22
  7.6 1.0 copy-done.6
  8.6 1.0 fusion.5.sact_ref
  9.6 123.1 %shard_map.176 = (bf16[256,2048]{1,0:T(8,128)(2,1)}, bf16[8,128,512]{2,1,0:T(8,128)(2,1)}, f32[8,16,256]{2,1,0:T(8,128)}, bf16[4,256,512]{2,1,0:T(8,128)(2,1)}) custom-call(bf16[256,2048]{1,0:T(8,128)(2,1)} %copy-done.1, f32[16,256]{1,0:T(8,128)} %pad_maximum_fusion.1.side_ref, bf16[128,512]{1,0:T(8,128)(2,1)} %pad_maximum_fusion.kv_ref, ...), custom_call_target="tpu_custom_call" | custom-call | tf_op jit(solution)/shard_map/pallas_call | solution.py:521
  132.7 0.8 slice_bitcast_fusion
  133.5 0.3 reduce_window_sum.13
  133.8 0.2 slice_reduce_fusion
  134.0 0.1 select_reduce_fusion.2
  134.1 0.1 broadcast_select_fusion
  134.2 1.9 %select_reduce_fusion = f32[128]{0:T(128)S(1)} fusion(f32[8,128]{1,0:T(8,128)S(1)} %bitcast.56, f32[128]{0:T(128)S(1)} %fusion.20, pred[8]{0:T(512)(128)(4,1)S(1)} %get-tuple-element.15, pred[128,128]{1,0:T(8,128)(4,1)S(1)} %iota_compare_fusion, pred[8]{0:T(512)(128)(4,1)S(1)} %get-tuple-element.14), kind=kLoop, calls=%fused_computation.14 | loop fusion | flops 655232 | bytes 21520 | tf_op jit(solution)/shard_map/reduce_max | solution.py:70
  136.1 0.6 fusion.14
  136.7 0.7 bitcast_maximum_fusion
  137.3 0.1 broadcast_bitcast_fusion
  137.4 0.1 broadcast_bitcast_fusion.1
  137.5 0.1 and.56
  137.6 0.0 copy-start.8
  137.6 1.6 %fusion.21 = (f32[128]{0:T(128)S(1)}, bf16[128,1024]{1,0:T(8,128)(2,1)S(1)}) fusion(f32[128]{0:T(128)S(1)} %bitcast_maximum_fusion, f32[1024]{0:T(1024)S(1)} %bitcast.57, f32[128]{0:T(128)S(1)} %fusion.20, pred[16,8,8,128]{3,2,1,0:T(8,128)(4,1)S(1)} %bitcast.53, pred[1024]{0:T(1024)(128)(4,1)S(1)} %broadcast_bitcast_fusion, ...), kind=kOutput, calls=%fused_computation.57 | convolution fusion | flops 68288384 | bytes 990724 | tf_op jit(solution)/shard_map/td,sd->ts/dot_general | solution.py:73
  139.2 0.9 fusion.6.gated_ref
  140.1 14.6 %shard_map.177 = bf16[128,2048]{1,0:T(8,128)(2,1)} custom-call(bf16[128,256]{1,0:T(8,128)(2,1)} %fusion.6.gated_ref, bf16[4,256,512]{2,1,0:T(8,128)(2,1)} %get-tuple-element.8.mwq_ref), custom_call_target="tpu_custom_call" | custom-call | tf_op jit(solution)/shard_map/pallas_call | solution.py:568
  154.7 1.9 %copy.27 = bf16[128,2048]{1,0:T(8,128)(2,1)} copy(bf16[128,2048]{1,0:T(8,128)(2,1)} %shard_map.177) | data formatting | bytes 1048576
  156.6 1.0 copy.28
  (21 shorter events, 0.1 us)
Async XLA Ops:
  0.6 6.5 %copy-start = (bf16[2048,128]{1,0:T(8,128)(2,1)S(1)}, bf16[2048,128]{1,0:T(8,128)(2,1)}, u32[]{:S(2)}) copy-start(bf16[2048,128]{1,0:T(8,128)(2,1)} %param.31) | copy-start | bytes 1572868
  0.6 6.2 %copy-start.2 = (bf16[256,2048]{1,0:T(8,128)(2,1)S(1)}, bf16[256,2048]{1,0:T(8,128)(2,1)}, u32[]{:S(2)}) copy-start(bf16[256,2048]{1,0:T(8,128)(2,1)} %param.24) | copy-start | bytes 3145732
  0.7 6.2 %copy-start.4 = (f32[2048]{0:T(1024)S(1)}, f32[2048]{0:T(1024)}, u32[]{:S(2)}) copy-start(f32[2048]{0:T(1024)} %param.25) | copy-start | bytes 24580
  7.1 2.5 %copy-start.1 = (bf16[256,2048]{1,0:T(8,128)(2,1)}, bf16[256,2048]{1,0:T(8,128)(2,1)S(1)}, u32[]{:S(2)}) copy-start(bf16[256,2048]{1,0:T(8,128)(2,1)S(1)} %fusion.2.x_ref) | copy-start | bytes 3145732
  7.2 1.4 copy-start.6
  9.6 127.9 %copy-start.7 = (bf16[128,512]{1,0:T(8,128)(2,1)S(1)}, bf16[128,512]{1,0:T(8,128)(2,1)}, u32[]{:S(2)}) copy-start(bf16[128,512]{1,0:T(8,128)(2,1)} %param.17) | copy-start | bytes 393220
  137.6 1.6 %copy-start.5 = (bf16[8,128,512]{2,1,0:T(8,128)(2,1)S(1)}, bf16[8,128,512]{2,1,0:T(8,128)(2,1)}, u32[]{:S(2)}) copy-start(bf16[8,128,512]{2,1,0:T(8,128)(2,1)} %get-tuple-element.6) | copy-start | bytes 3145732
  137.6 1.6 %copy-start.8 = (bf16[128,256]{1,0:T(8,128)(2,1)S(1)}, bf16[128,256]{1,0:T(8,128)(2,1)}, u32[]{:S(2)}) copy-start(bf16[128,256]{1,0:T(8,128)(2,1)} %param.20) | copy-start | bytes 196612
  140.1 16.5 %copy-start.3 = (bf16[256,2048]{1,0:T(8,128)(2,1)S(1)}, bf16[256,2048]{1,0:T(8,128)(2,1)}, u32[]{:S(2)}) copy-start(bf16[256,2048]{1,0:T(8,128)(2,1)} %get-tuple-element.21) | copy-start | bytes 3145732
where the time goes:
time: 158 us
  Pallas kernels  138 us (87%)
  other arithmetic  9.1 us (6%)
  local copies, waits for them, and re-layouts  6.01 us (4%)
  matrix products  3.93 us (2%)
    pallas_call x1, Pallas kernels, dense_experts(): pl.pallas_call(functools.partial(dense_kernel, lines, teams), out_shape=(...  123 us
    pallas_call x1, Pallas kernels, dense_experts(): pl.pallas_call(functools.partial(project_kernel, teams), out_shape=jax.Sh...  14.6 us
    unnamed x20, local copies, waits for them, and re-layouts  3.89 us

commit v1 on v0

v1 whole, which is shorter than its diff:
```python
import functools

import jax
import jax.numpy as jnp
from jax import lax
from jax.experimental import pallas as pl
from jax.experimental.pallas import tpu as pltpu
from jax.sharding import PartitionSpec as P

D = 2048
MEMORY_HEADS = 2
KEY_DIM = 256
BLOCK = 128
FF = 1024


epsilon = 1e-06
lowest = -1e30
den_floor = 4.0


def mixer_local(queries, key_vectors, values, input_gate, forget_gate):
    tp_count = lax.axis_size("tp")
    tp_rank = lax.axis_index("tp")
    head_index = tp_rank // (tp_count // MEMORY_HEADS)
    offset = head_index * KEY_DIM
    query_head = lax.dynamic_slice_in_dim(queries, offset, KEY_DIM, 1)
    key_head = lax.dynamic_slice_in_dim(key_vectors, offset, KEY_DIM, 1)
    select = jnp.arange(MEMORY_HEADS, dtype=jnp.int32)[None, :] == head_index
    gates = jnp.stack(
        [
            jnp.sum(jnp.where(select, input_gate, 0.0), axis=1),
            jax.nn.log_sigmoid(jnp.sum(jnp.where(select, forget_gate, 0.0), axis=1)),
        ]
    )
    return query_head, jnp.concatenate([key_head, values], axis=1), gates


def mixer_rows(query_head, both, gates, out_gate):
    ep_count = lax.axis_size("ep")
    ep_rank = lax.axis_index("ep")
    length = query_head.shape[0]
    factor = KEY_DIM ** (-0.5)
    keys_all = both[:, :KEY_DIM]
    values_all = both[:, KEY_DIM:]
    total = ep_count * length
    blocks = total // BLOCK
    mine = length // BLOCK
    input_all = gates[0].reshape(blocks, BLOCK)
    cumulative = jnp.cumsum(gates[1].reshape(blocks, BLOCK), axis=1)
    block_total = cumulative[:, -1]
    index = jnp.arange(blocks, dtype=jnp.int32)
    here = ep_rank * mine + jnp.arange(mine, dtype=jnp.int32)
    between = (index[None, None, :] > index[None, :, None]) & (
        index[None, None, :] < here[:, None, None]
    )
    gap = jnp.sum(jnp.where(between, block_total[None, None, :], 0.0), axis=2)
    ahead = jnp.sum(jnp.where(index[None, :] < here[:, None], block_total[None, :], 0.0), axis=1)
    keep = block_total[:, None] - cumulative + input_all
    own_cumulative = lax.dynamic_slice_in_dim(cumulative, ep_rank * mine, mine, 0)
    same = index[None, :] == here[:, None]
    column = jnp.where(same[:, :, None], input_all - cumulative, keep + gap[:, :, None])
    log_weight = own_cumulative[:, :, None, None] + column[:, None]
    row_at = jnp.arange(BLOCK, dtype=jnp.int32)
    visible = (index[None, :] < here[:, None])[:, None, :, None] | (
        same[:, None, :, None] & (row_at[None, :, None, None] >= row_at[None, None, None, :])
    )
    log_weight = jnp.where(visible, log_weight, -jnp.inf).reshape(length, total)
    carried = (own_cumulative + ahead[:, None]).reshape(length)
    stabilizer = jnp.maximum(carried, jnp.max(log_weight, axis=1))
    within = jnp.exp(log_weight - stabilizer[:, None])
    scores = (
        jnp.einsum("td,sd->ts", query_head, keys_all, preferred_element_type=jnp.float32) * factor
    )
    weights = scores * within
    numerator = jnp.dot(
        weights.astype(jnp.bfloat16), values_all, preferred_element_type=jnp.float32
    )
    denominator = jnp.sum(weights, axis=1)
    hidden = numerator / jnp.maximum(jnp.abs(denominator), den_floor)[:, None]
    gated_rows = (hidden * jax.nn.sigmoid(out_gate.astype(jnp.float32))).astype(jnp.bfloat16)
    return gated_rows


splits = ((64, 16), (64, 16))
halves = 2


def lane_kernel(
    lines,
    ig_ref, fg_ref, gain_ref, ids_ref, rw_ref,
    q_ref, k_ref, v_ref, og_ref, mw_ref, x_ref, g_ref, u_ref, d_ref, sg_ref, su_ref, sd_ref,
    mo_ref, eo_ref,
    xbuf, qb, ogb, mwb, gall, uall, dall, sgall, suall, sdall, sall,
    tok, act, kvb, side, brow, stab, num, den, res, xin, zout, zin, mpart, mpeer, msum, mother,
    local, z_send, z_recv, x_send, x_recv, e_send, e_recv, kz_send, kz_recv, kx_send, kx_recv,
    s_send, s_recv, a_send, a_recv, b_send, b_recv, y_send, y_recv, f_send, f_recv,
    xo_send, xo_recv, zo_send, zo_recv, ey_send, ey_recv, eb_send, eb_recv, ef_send, ef_recv,
    m_send, m_recv,
):
    me = lax.axis_index("ep")
    j = lax.axis_index("tp")
    z, x = me // 2, me % 2
    y, c = j // 2, j % 2
    ep_count = 2 * lines
    rows = x_ref.shape[0] // 2
    length = q_ref.shape[0]
    key_dim = qb.shape[1]
    half = dall.shape[2]
    units = g_ref.shape[2]
    shared = sg_ref.shape[1]
    piece = half // halves
    part = length // 2
    low, wide = jnp.bfloat16, jnp.float32

    def remote(src, dst, send, recv, ep, tp):
        return pltpu.make_async_remote_copy(
            src_ref=src, dst_ref=dst, send_sem=send, recv_sem=recv,
            device_id={"ep": ep, "tp": tp}, device_id_type=pl.DeviceIdType.MESH,
        )

    across = z * 2 + 1 - x
    other_y = (1 - y) * 2 + c
    buddy = y * 2 + 1 - c

    def lanes(start, size):
        return pl.ds(pl.multiple_of(start, 128), size)

    def sublanes(start, size):
        return pl.ds(pl.multiple_of(start, 8), size)

    mine = lanes(y * half, half)
    theirs = lanes((1 - y) * half, half)
    heads = lanes(y * key_dim, key_dim)

    def load(n):
        pairs = (
            (x_ref.at[sublanes(c * rows, rows)], xbuf),
            (g_ref.at[0], gall.at[c]),
            (u_ref.at[0], uall.at[c]),
            (k_ref.at[:, heads], kvb.at[me, :, :key_dim]),
            (v_ref, kvb.at[me, :, key_dim:]),
            (d_ref.at[0, :, mine], dall.at[y, sublanes(c * units, units)]),
            (q_ref.at[:, heads], qb),
            (og_ref, ogb),
            (sg_ref, sgall.at[c]),
            (su_ref, suall.at[c]),
            (sd_ref.at[:, mine], sdall.at[y, sublanes(c * shared, shared)]),
            (mw_ref, mwb),
        )
        return pltpu.make_async_copy(*pairs[n], local.at[n])

    for n in range(12):
        load(n).start()

    barrier = pltpu.get_barrier_semaphore()

    def greet(ep, tp):
        pl.semaphore_signal(
            barrier, inc=1, device_id={"ep": ep, "tp": tp}, device_id_type=pl.DeviceIdType.MESH
        )

    for k in range(1, ep_count):
        greet(lax.rem(me + k, ep_count), j)
    greet(me, other_y)
    greet(me, buddy)

    bounds = []
    at = 0
    for size, only in splits:
        bounds.append((at, size, only))
        at += size

    def z_copy(zb, way, n):
        start, size, _ = bounds[n]
        ref = tok.at[zb * 2 + x, start : start + size]
        to = z + 1 - 2 * way
        return remote(ref, ref, z_send.at[way, zb, n], z_recv.at[zb, n], to * 2 + x, j)

    def x_copy(zb, column, n):
        start, size, only = bounds[n]
        ref = tok.at[zb * 2 + column, sublanes(start + y * only, size - only)]
        return remote(ref, ref, x_send.at[zb, n], x_recv.at[zb, n], across, j)

    def x_arrival(zb, n):
        start, size, only = bounds[n]
        ref = tok.at[zb * 2 + 1 - x, sublanes(start + y * only, size - only)]
        return remote(ref, ref, x_send.at[zb, n], x_recv.at[zb, n], across, j)

    def e_copy(zb, n):
        start, size, only = bounds[n]
        ref = tok.at[zb * 2 + 1 - x, sublanes(start + y * (size - only), only)]
        return remote(ref, ref, e_send.at[zb, n], e_recv.at[zb, n], me, other_y)

    def kz_copy(zb):
        ref = kvb.at[zb * 2 + x]
        return remote(ref, ref, kz_send.at[zb], kz_recv.at[zb], (z + 1) * 2 + x, j)

    def kx_copy(zb, column):
        ref = kvb.at[zb * 2 + column]
        return remote(ref, ref, kx_send.at[zb], kx_recv.at[zb], across, j)

    def s_copy(k):
        return remote(
            side.at[me], side.at[me], s_send.at[k - 1], s_recv.at[me], lax.rem(me + k, ep_count), j
        )

    def s_arrival(k):
        source = lax.rem(me + k, ep_count)
        return remote(
            side.at[source], side.at[source], s_send.at[k - 1], s_recv.at[source], source, j
        )

    def a_copy(block, team):
        ref = act.at[block, team]
        return remote(ref, ref, a_send.at[block], a_recv.at[block], me, other_y)

    def b_copy(core, n):
        pairs = (
            (g_ref.at[0], gall.at[core]),
            (u_ref.at[0], uall.at[core]),
            (sg_ref, sgall.at[core]),
            (su_ref, suall.at[core]),
            (d_ref.at[0, :, mine], dall.at[y, sublanes(core * units, units)]),
            (sd_ref.at[:, mine], sdall.at[y, sublanes(core * shared, shared)]),
        )
        return remote(*pairs[n], b_send.at[n], b_recv.at[n], me, buddy)

    def y_copy(team, n):
        pairs = (
            (d_ref.at[0, :, theirs], dall.at[team, sublanes(c * units, units)]),
            (sd_ref.at[:, theirs], sdall.at[team, sublanes(c * shared, shared)]),
            (sall.at[team], sall.at[team]),
        )
        return remote(*pairs[n], y_send.at[n], y_recv.at[n], me, other_y)

    def f_copy(core, n):
        refs = (
            dall.at[1 - y, sublanes(core * units, units)],
            sdall.at[1 - y, sublanes(core * shared, shared)],
        )
        return remote(refs[n], refs[n], f_send.at[n], f_recv.at[n], me, buddy)

    def xo_copy(zb, n):
        cols = pl.ds(n * piece, piece)
        return remote(
            res.at[zb * 2 + 1 - x, :, cols], xin.at[zb, :, cols],
            xo_send.at[zb, n], xo_recv.at[zb, n], across, j,
        )

    def zo_copy(zb, n):
        cols = pl.ds(n * piece, piece)
        return remote(
            zout.at[zb, :, cols], zin.at[z, :, cols],
            zo_send.at[zb, n], zo_recv.at[z, n], zb * 2 + x, j,
        )

    def zo_arrival(zb, n):
        cols = pl.ds(n * piece, piece)
        return remote(
            zout.at[zb, :, cols], zin.at[zb, :, cols],
            zo_send.at[zb, n], zo_recv.at[zb, n], zb * 2 + x, j,
        )

    def final(core, team, n):
        return eo_ref.at[
            sublanes(core * rows, rows), lanes(team * half + n * piece, piece)
        ]

    def ey_copy(team, n):
        ref = final(c, team, n)
        return remote(ref, ref, ey_send.at[n], ey_recv.at[n], me, other_y)

    def eb_copy(core, n):
        ref = final(core, y, n)
        return remote(ref, ref, eb_send.at[n], eb_recv.at[n], me, buddy)

    def ef_copy(core, n):
        ref = final(core, 1 - y, n)
        return remote(ref, ref, ef_send.at[n], ef_recv.at[n], me, buddy)

    def m_copy(core, n):
        ref = mo_ref.at[sublanes(core * part, part)]
        pairs = (
            (mpart.at[sublanes((1 - c) * part, part)], mpeer, buddy),
            (msum, mother, other_y),
            (ref, ref, buddy),
        )
        source, target, to = pairs[n]
        return remote(source, target, m_send.at[n], m_recv.at[n], me, to)

    at_row = lax.broadcasted_iota(jnp.int32, (length, length), 0)
    at_lane = lax.broadcasted_iota(jnp.int32, (length, length), 1)
    token_lanes = lanes(c * rows, rows)
    ids = ids_ref[:, token_lanes]
    route = rw_ref[:, token_lanes]
    for e in range(ep_count):
        side[me, e : e + 1, :] = jnp.sum(jnp.where(ids == e, route, 0.0), axis=0, keepdims=True)
    forget = fg_ref[pl.ds(y, 1), :]
    small = jnp.exp(-jnp.abs(forget))
    kept = jnp.minimum(forget, 0.0) - jnp.log1p(small)
    kept_column = jnp.sum(jnp.where(at_row == at_lane, kept, 0.0), axis=1, keepdims=True)
    cumulative = jnp.sum(jnp.where(at_row <= at_lane, kept_column, 0.0), axis=0, keepdims=True)
    side[me, ep_count : ep_count + 1, :] = ig_ref[pl.ds(y, 1), :] - cumulative
    side[me, ep_count + 1 : ep_count + 2, :] = jnp.broadcast_to(
        jnp.sum(kept, axis=1, keepdims=True), (1, length)
    )

    def normalize(start, size):
        def group(n, carry):
            at_rows = sublanes(start + n * 16, 16)
            wide_rows = xbuf[at_rows, :].astype(wide)
            scale = lax.rsqrt(jnp.mean(wide_rows * wide_rows, axis=1, keepdims=True) + epsilon)
            tok[me, at_rows, :] = (wide_rows * scale * gain_ref[...]).astype(low)
            return carry

        lax.fori_loop(0, size // 16, group, 0)

    def can_go(way):
        to = z + 1 - 2 * way
        return (to >= 0) & (to < lines)

    load(0).wait()
    normalize(bounds[0][0], bounds[0][1])
    pl.semaphore_wait(barrier, ep_count + 1)
    for n in range(len(bounds)):
        if n:
            normalize(bounds[n][0], bounds[n][1])
        for way in range(2):

            @pl.when(can_go(way))
            def _():
                z_copy(z, way, n).start()

        x_copy(z, x, n).start()
        if n == 0:
            for i in range(6):
                b_copy(c, i).start()
            y_copy(y, 0).start()
    for k in range(1, ep_count):
        s_copy(k).start()
    load(3).wait()
    load(4).wait()

    @pl.when(z + 1 < lines)
    def _():
        kz_copy(z).start()

    @pl.when(x == 0)
    def _():
        kx_copy(z, x).start()

    load(1).wait()
    load(2).wait()
    b_copy(1 - c, 0).wait_recv()
    b_copy(1 - c, 1).wait_recv()

    def activate(block):
        for h in range(2):
            gate = jnp.dot(tok[block], gall[h], preferred_element_type=wide)
            up = jnp.dot(tok[block], uall[h], preferred_element_type=wide)
            act[block, y, :, h * units : (h + 1) * units] = (
                gate / (1.0 + jnp.exp(-gate)) * up
            ).astype(low)
        a_copy(block, y).start()

    def valid(s, d, zb):
        return (s >= 0) & (s < lines) & (zb >= 0) & (zb < lines) & ((s > 0) | (d == 0))

    def both_ways(s, work):
        def one(d, carry):
            zb = z + s * (2 * d - 1)

            @pl.when(valid(s, d, zb))
            def _():
                work(d, zb)

            return carry

        lax.fori_loop(0, 2, one, 0)

    def forward(d, zb):
        for n in range(len(bounds)):
            z_copy(zb, d, n).wait_recv()

            @pl.when(can_go(d))
            def _():
                z_copy(zb, d, n).start()

            x_copy(zb, x, n).start()

        @pl.when(d == 0)
        def _():
            kz_copy(zb).wait_recv()

            @pl.when(z + 1 < lines)
            def _():
                kz_copy(zb).start()

            kx_copy(zb, x).start()

    def pass_on(d, zb):
        for n in range(len(bounds)):
            x_arrival(zb, n).wait_recv()
            if bounds[n][2]:
                e_copy(zb, n).start()

    def near(d, zb):
        activate(zb * 2 + x)

    def far(d, zb):
        for n in range(len(bounds)):
            if bounds[n][2]:
                e_copy(zb, n).wait_recv()
        activate(zb * 2 + 1 - x)

    def finish(block):
        a_copy(block, 1 - y).wait_recv()
        weight = jnp.sum(
            jnp.where(at_row == at_lane, side[block, pl.ds(me, 1), :], 0.0), axis=1, keepdims=True
        )
        for n in range(halves):
            cols = slice(n * piece, (n + 1) * piece)
            total = jnp.dot(act[block, 0], dall[0, :, cols], preferred_element_type=wide)
            total += jnp.dot(act[block, 1], dall[1, :, cols], preferred_element_type=wide)
            res[block, :, cols] = (total * weight).astype(low)

    def finish_near(d, zb):
        finish(zb * 2 + x)

    def finish_far(d, zb):
        finish(zb * 2 + 1 - x)
        for n in range(halves):
            xo_copy(zb, n).start()

    def send_home(d, zb):
        for n in range(halves):
            cols = slice(n * piece, (n + 1) * piece)
            xo_copy(zb, n).wait_recv()
            zout[zb, :, cols] = (
                res[zb * 2 + x, :, cols].astype(wide) + xin[zb, :, cols].astype(wide)
            ).astype(low)
            zo_copy(zb, n).start()

    def memory(d, zb):
        @pl.when((d == 0) & (zb * 2 + 1 - x < me))
        def _():
            kx_copy(zb, 1 - x).wait_recv()

        def one(n, carry):
            block = zb * 2 + n

            @pl.when((d == 0) & (block <= me))
            def _():
                scores = lax.dot_general(
                    qb[...], kvb[block, :, :key_dim], (((1,), (1,)), ((), ())),
                    preferred_element_type=wide,
                ) * (key_dim ** -0.5)
                seen = (block < me) | (at_row >= at_lane)
                shown = jnp.where(seen, brow[block, 0:1, :] - stab[...], lowest)
                weights = jnp.where(seen, scores * jnp.exp(shown), 0.0)
                num[...] += jnp.dot(
                    weights.astype(low), kvb[block, :, key_dim:], preferred_element_type=wide
                )
                den[...] += jnp.broadcast_to(
                    jnp.sum(weights, axis=1, keepdims=True), den.shape
                )

            return carry

        lax.fori_loop(0, 2, one, 0)

    def prepare():
        for k in range(1, ep_count):
            s_arrival(k).wait_recv()
        gap = jnp.zeros((1, length), wide)
        top = jnp.full((1, length), lowest, wide)
        for b in reversed(range(ep_count)):
            earlier = b < me
            gap = jnp.where(earlier, gap + side[b, ep_count + 1 : ep_count + 2, :], gap)
            row = side[b, ep_count : ep_count + 1, :] + gap
            brow[b, 0:1, :] = row
            top = jnp.where(earlier, jnp.maximum(top, row), top)
        own = side[me, ep_count : ep_count + 1, :]
        within = jnp.max(
            jnp.where(at_row >= at_lane, own, lowest), axis=1, keepdims=True
        )
        before = jnp.max(jnp.maximum(top, gap), axis=1, keepdims=True)
        stab[...] = jnp.broadcast_to(jnp.maximum(within, before), stab.shape)
        num[...] = jnp.zeros_like(num)
        den[...] = jnp.zeros_like(den)
        load(6).wait()
        load(8).wait()
        load(9).wait()
        for n in (2, 3):
            b_copy(1 - c, n).wait_recv()
        for h in range(2):
            gate = jnp.dot(tok[me], sgall[h], preferred_element_type=wide)
            up = jnp.dot(tok[me], suall[h], preferred_element_type=wide)
            sall[y, :, h * shared : (h + 1) * shared] = (
                gate / (1.0 + jnp.exp(-gate)) * up
            ).astype(low)
        for n in (1, 2):
            y_copy(y, n).start()
        load(5).wait()
        y_copy(1 - y, 0).wait_recv()
        f_copy(c, 0).start()
        b_copy(1 - c, 4).wait_recv()
        f_copy(1 - c, 0).wait_recv()

    def step(t, carry):
        both_ways(jnp.where(t > 0, t, lines), forward)
        both_ways(jnp.where(t > 2, t - 2, lines), finish_far)
        both_ways(t - 1, pass_on)
        both_ways(t, near)
        both_ways(jnp.where(t > 3, t - 3, lines), send_home)
        both_ways(t - 1, far)

        @pl.when(t == 1)
        def _():
            prepare()

        both_ways(t - 1, memory)
        both_ways(t - 1, finish_near)
        return carry

    lax.fori_loop(0, lines + 1, step, 0)

    def late(n, carry):
        both_ways(jnp.where(n == 0, lines - 1, 0), finish_far)

        @pl.when(n == 0)
        def _():
            both_ways(lines - 2, send_home)

        return carry

    lax.fori_loop(0, 2, late, 0)

    load(7).wait()
    load(11).wait()
    hidden = num[...] / jnp.maximum(jnp.abs(den[:, 0:1]), den_floor)
    gated = (hidden * (1.0 / (1.0 + jnp.exp(-ogb[...].astype(wide))))).astype(low)
    for n in range(4):
        cols = slice(n * half // 2, (n + 1) * half // 2)
        mpart[:, cols] = jnp.dot(gated, mwb[:, cols], preferred_element_type=wide).astype(low)
    m_copy(c, 0).start()
    load(10).wait()
    y_copy(1 - y, 1).wait_recv()
    f_copy(c, 1).start()
    y_copy(1 - y, 2).wait_recv()
    b_copy(1 - c, 5).wait_recv()
    m_copy(c, 0).wait_recv()
    msum[...] = (
        mpart[sublanes(c * part, part), :].astype(wide) + mpeer[...].astype(wide)
    ).astype(low)
    m_copy(c, 1).start()
    both_ways(lines - 1, send_home)
    f_copy(1 - c, 1).wait_recv()
    m_copy(c, 1).wait_recv()
    mo_ref[sublanes(c * part, part), :] = (
        msum[...].astype(wide) + mother[...].astype(wide)
    ).astype(low)
    m_copy(c, 2).start()

    for n in range(halves):
        cols = slice(n * piece, (n + 1) * piece)
        xo_copy(z, n).wait_recv()
        total = res[me, :, cols].astype(wide) + xin[z, :, cols].astype(wide)
        for team in range(2):
            total += jnp.dot(sall[team], sdall[team, :, cols], preferred_element_type=wide)
        for k in range(1, lines):
            source = lax.rem(z + k, lines)
            zo_arrival(source, n).wait_recv()
            total += zin[source, :, cols].astype(wide)
        eo_ref[sublanes(c * rows, rows), lanes(y * half + n * piece, piece)] = total.astype(low)
        ey_copy(y, n).start()
        eb_copy(c, n).start()
    for n in range(halves):
        ey_copy(1 - y, n).wait_recv()
        ef_copy(c, n).start()
    m_copy(1 - c, 2).wait_recv()
    for n in range(halves):
        eb_copy(1 - c, n).wait_recv()
        ef_copy(1 - c, n).wait_recv()

    for n in range(6):
        b_copy(c, n).wait_send()
    for n in range(3):
        y_copy(y, n).wait_send()
        m_copy(c, n).wait_send()
    for n in range(2):
        f_copy(c, n).wait_send()
    for n in range(halves):
        ey_copy(y, n).wait_send()
        eb_copy(c, n).wait_send()
        ef_copy(c, n).wait_send()
    for k in range(1, ep_count):
        s_copy(k).wait_send()

    @pl.when(x == 0)
    def _():
        kx_copy(z, x).wait_send()

    def drain(zb, carry):
        for way in range(2):
            passing = (zb <= z) if way == 0 else (zb >= z)

            @pl.when(can_go(way) & passing)
            def _():
                for n in range(len(bounds)):
                    z_copy(zb, way, n).wait_send()

        @pl.when((z + 1 < lines) & (zb <= z))
        def _():
            kz_copy(zb).wait_send()

        @pl.when(zb < z)
        def _():
            kx_copy(zb, x).wait_send()

        for n in range(len(bounds)):
            x_copy(zb, x, n).wait_send()
            if bounds[n][2]:
                e_copy(zb, n).wait_send()
        for n in range(halves):
            xo_copy(zb, n).wait_send()

            @pl.when(zb != z)
            def _():
                zo_copy(zb, n).wait_send()

        for n in range(2):
            a_copy(zb * 2 + n, y).wait_send()
        return carry

    lax.fori_loop(0, lines, drain, 0)


def lane_program(
    queries, key_vectors, values, out_gate, input_gate, forget_gate, mix_weight,
    expert_input, norm_gain, route_ids, route_weights, expert_gate, expert_up, expert_down,
    shared_gate, shared_up, shared_down,
):
    ep_count = lax.axis_size("ep")
    lines = ep_count // 2
    tokens, width = expert_input.shape
    rows, half = tokens // 2, width // 2
    length, channels = values.shape
    units, shared = expert_gate.shape[2], shared_gate.shape[1]
    low, wide, dma = jnp.bfloat16, jnp.float32, pltpu.SemaphoreType.DMA
    side_rows = ep_count + 2 + -(ep_count + 2) % 8
    chunks = len(splits)
    vmem = pl.BlockSpec(memory_space=pltpu.VMEM)
    hbm = pl.BlockSpec(memory_space=pl.ANY)

    def buffer(*shape, dtype=low):
        return pltpu.VMEM(shape, dtype)

    return pl.pallas_call(
        functools.partial(lane_kernel, lines),
        out_shape=(
            jax.ShapeDtypeStruct((length, width), low),
            jax.ShapeDtypeStruct((tokens, width), low),
        ),
        in_specs=[vmem] * 5 + [hbm] * 12,
        out_specs=(vmem, vmem),
        scratch_shapes=[
            buffer(rows, width),
            buffer(length, KEY_DIM),
            buffer(length, channels),
            buffer(channels, width),
            buffer(2, width, units),
            buffer(2, width, units),
            buffer(2, 2 * units, half),
            buffer(2, width, shared),
            buffer(2, width, shared),
            buffer(2, 2 * shared, half),
            buffer(2, rows, 2 * shared),
            buffer(ep_count, rows, width),
            buffer(ep_count, 2, rows, 2 * units),
            buffer(ep_count, length, KEY_DIM + channels),
            buffer(ep_count, side_rows, rows, dtype=wide),
            buffer(ep_count, 8, length, dtype=wide),
            buffer(length, length, dtype=wide),
            buffer(length, channels, dtype=wide),
            buffer(length, 128, dtype=wide),
            buffer(ep_count, rows, half),
            buffer(lines, rows, half),
            buffer(lines, rows, half),
            buffer(lines, rows, half),
            buffer(length, width),
            buffer(length // 2, width),
            buffer(length // 2, width),
            buffer(length // 2, width),
            dma((12,)),
            dma((2, lines, chunks)), dma((lines, chunks)),
            dma((lines, chunks)), dma((lines, chunks)),
            dma((lines, chunks)), dma((lines, chunks)),
            dma((lines,)), dma((lines,)), dma((lines,)), dma((lines,)),
            dma((ep_count - 1,)), dma((ep_count,)),
            dma((ep_count,)), dma((ep_count,)),
            dma((6,)), dma((6,)), dma((3,)), dma((3,)), dma((2,)), dma((2,)),
            dma((lines, halves)), dma((lines, halves)),
            dma((lines, halves)), dma((lines, halves)),
            dma((halves,)), dma((halves,)), dma((halves,)), dma((halves,)),
            dma((halves,)), dma((halves,)),
            dma((3,)), dma((3,)),
        ],
        compiler_params=pltpu.CompilerParams(
            collective_id=0, has_side_effects=True, vmem_limit_bytes=56 * 1024 * 1024
        ),
    )(
        input_gate.T, forget_gate.T, norm_gain[None, :], route_ids.T, route_weights.T,
        queries, key_vectors, values, out_gate, mix_weight, expert_input,
        expert_gate, expert_up, expert_down, shared_gate, shared_up, shared_down,
    )


def expert_half(
    expert_input,
    norm_gain,
    route_ids,
    route_weights,
    expert_gate,
    expert_up,
    expert_down,
    shared_gate,
    shared_up,
    shared_down,
):
    ep_count = lax.axis_size("ep")
    tp_count = lax.axis_size("tp")
    tp_rank = lax.axis_index("tp")
    tokens = expert_input.shape[0]
    top_count = route_ids.shape[1]
    slice_units = expert_gate.shape[2]
    group_size = FF // slice_units
    per_ep = tp_count // group_size
    team_index = tp_rank // group_size
    expert_count = ep_count * per_ep
    capacity = 2 * tokens * top_count // expert_count
    rows_wide = expert_input.astype(jnp.float32)
    normed = (
        rows_wide
        * lax.rsqrt(jnp.mean(rows_wide * rows_wide, axis=-1, keepdims=True) + epsilon)
        * norm_gain
    ).astype(jnp.bfloat16)
    chosen = route_ids.reshape(-1)
    onehot = (chosen[:, None] == jnp.arange(expert_count, dtype=jnp.int32)[None, :]).astype(
        jnp.int32
    )
    slot_rank = jnp.sum((jnp.cumsum(onehot, axis=0) - onehot) * onehot, axis=1)
    in_team = chosen % per_ep == team_index
    target = jnp.where(in_team, chosen // per_ep * capacity + slot_rank, ep_count * capacity)
    token_of = jnp.arange(chosen.shape[0], dtype=jnp.int32) // top_count
    slot_token = jnp.zeros((ep_count * capacity,), jnp.int32).at[target].set(token_of, mode="drop")
    slot_live = jnp.zeros((ep_count * capacity,), jnp.int32).at[target].set(1, mode="drop")
    outgoing = jnp.where(slot_live[:, None] > 0, normed[slot_token], jnp.zeros((), jnp.bfloat16))
    outgoing = outgoing.reshape(ep_count, capacity, D)
    gate_slice = expert_gate[0]
    up_slice = expert_up[0]
    down_slice = expert_down[0]
    arrived = lax.all_to_all(outgoing, "ep", split_axis=0, concat_axis=0, tiled=True)
    gate_val = jnp.einsum("sid,df->sif", arrived, gate_slice, preferred_element_type=jnp.float32)
    up_val = jnp.einsum("sid,df->sif", arrived, up_slice, preferred_element_type=jnp.float32)
    hidden = (jax.nn.silu(gate_val) * up_val).astype(jnp.bfloat16)
    partial_value = jnp.einsum(
        "sif,fd->sid", hidden, down_slice, preferred_element_type=jnp.float32
    )
    partial_value = partial_value.astype(jnp.bfloat16)
    returned = lax.all_to_all(partial_value, "ep", split_axis=0, concat_axis=0, tiled=True)
    flat_back = returned.reshape(ep_count * capacity, returned.shape[2])
    gather_at = jnp.where(in_team, target, 0).reshape(tokens, top_count)
    weight_at = jnp.where(in_team, route_weights.reshape(-1), 0.0).reshape(tokens, top_count)
    combined = jnp.zeros((tokens, returned.shape[2]), jnp.float32)
    for pick_index in range(top_count):
        combined = (
            combined
            + flat_back[gather_at[:, pick_index]].astype(jnp.float32)
            * weight_at[:, pick_index][:, None]
        )
    shared_gate_val = jnp.dot(normed, shared_gate, preferred_element_type=jnp.float32)
    shared_up_val = jnp.dot(normed, shared_up, preferred_element_type=jnp.float32)
    shared_act = (jax.nn.silu(shared_gate_val) * shared_up_val).astype(jnp.bfloat16)
    return combined + jnp.dot(shared_act, shared_down, preferred_element_type=jnp.float32)


def shards(
    queries,
    key_vectors,
    values,
    out_gate,
    input_gate,
    forget_gate,
    mix_weight,
    expert_input,
    norm_gain,
    route_ids,
    route_weights,
    expert_gate,
    expert_up,
    expert_down,
    shared_gate,
    shared_up,
    shared_down,
):
    ep_count, tp_count = lax.axis_size("ep"), lax.axis_size("tp")
    tokens, slots = expert_input.shape[0], route_ids.shape[1] * 2 * expert_input.shape[0]
    per_ep = tp_count * expert_gate.shape[2] // FF
    even = ep_count % 2 == 0 and tp_count == 4 and MEMORY_HEADS * 2 == tp_count
    blocked = values.shape[0] == BLOCK and tokens == 2 * BLOCK and ep_count > 2
    dense = even and blocked and per_ep == 1 and slots // (ep_count * per_ep) >= tokens
    experts = (
        expert_input,
        norm_gain,
        route_ids,
        route_weights,
        expert_gate,
        expert_up,
        expert_down,
        shared_gate,
        shared_up,
        shared_down,
    )
    if dense:
        return lane_program(
            queries, key_vectors, values, out_gate, input_gate, forget_gate, mix_weight, *experts
        )
    query_head, both, gates = mixer_local(
        queries, key_vectors, values, input_gate, forget_gate
    )
    both = lax.all_gather(both, "ep", axis=0, tiled=True)
    gates = lax.all_gather(gates, "ep", axis=1, tiled=True)
    gated_rows = mixer_rows(query_head, both, gates, out_gate)
    mixer_partial = jnp.dot(gated_rows, mix_weight, preferred_element_type=jnp.float32)
    expert_partial = expert_half(*experts)
    mixer_piece = lax.psum_scatter(
        mixer_partial.astype(jnp.bfloat16), "tp", scatter_dimension=0, tiled=True
    )
    mixer_out = lax.all_gather(mixer_piece, "tp", axis=0, tiled=True)
    expert_piece = lax.psum_scatter(expert_partial, "tp", scatter_dimension=0, tiled=True).astype(
        jnp.bfloat16
    )
    expert_out = lax.all_gather(expert_piece, "tp", axis=0, tiled=True)
    return (mixer_out, expert_out)


def solution(mesh):
    return jax.shard_map(
        shards,
        mesh=mesh,
        in_specs=(
            P("ep", None),
            P("ep", None),
            P("ep", "tp"),
            P("ep", "tp"),
            P("ep", None),
            P("ep", None),
            P("tp", None),
            P("ep", None),
            P(),
            P("ep", None),
            P("ep", None),
            P(("ep", "tp"), None, None),
            P(("ep", "tp"), None, None),
            P(("ep", "tp"), None, None),
            P(None, "tp"),
            P(None, "tp"),
            P("tp", None),
        ),
        out_specs=(P("ep", None), P("ep", None)),
        check_vma=False,
    )
```

time: 158 us -> 101 us (0.64)
  the two profiles are of different devices: /device:TPU:25 before, /device:TPU:0 now
where the time goes in v1:
time: 101 us
  Pallas kernels  97.1 us (96%)
  local copies, waits for them, and re-layouts  2.94 us (3%)
    pallas_call x1, Pallas kernels, lane_program(): pl.pallas_call(functools.partial(lane_kernel, lines), out_shape=(jax.Shap...  97.1 us
    unnamed x4, local copies, waits for them, and re-layouts  2.94 us

profile of v1, /device:TPU:0, one launch (start us, length us, event | category | flops | bytes accessed | tf_op | source)
XLA Modules:
  0.0 100.7 jit_solution(10429756941932810594)
XLA Ops:
  0.6 97.1 %shard_map.176 = (bf16[128,2048]{1,0:T(8,128)(2,1)}, bf16[256,2048]{1,0:T(8,128)(2,1)}) custom-call(f32[2,128]{1,0:T(2,128)} %bitcast.8, f32[2,128]{1,0:T(2,128)} %bitcast.9, f32[1,2048]{1,0:T(1,128)} %bitcast.5, s32[4,256]{1,0:T(4,128)} %bitcast.6, f32[4,256]{1,0:T(4,128)} %bitcast.7, bf16[128,512]{1,0:T(8,128)(2,1)} %q_ref.1, bf16[128,512]{1,0:T(8,128)(2,1)} %k_ref.1, ...), custom_call_target="tpu_custom_call" | custom-call | tf_op jit(solution)/shard_map/pallas_call | solution.py:660
  97.7 0.0 copy-start
  97.8 2.0 %copy.21 = bf16[128,2048]{1,0:T(8,128)(2,1)} copy(bf16[128,2048]{1,0:T(8,128)(2,1)} %get-tuple-element.4) | data formatting | bytes 1048576
  99.7 0.0 copy-done
  99.7 1.0 copy.22
Async XLA Ops:
  97.7 2.0 %copy-start = (bf16[256,2048]{1,0:T(8,128)(2,1)S(1)}, bf16[256,2048]{1,0:T(8,128)(2,1)}, u32[]{:S(2)}) copy-start(bf16[256,2048]{1,0:T(8,128)(2,1)} %get-tuple-element.5) | copy-start | bytes 3145732

commit v2 on v1

--- a/solution.py
+++ b/solution.py
@@ -82,12 +82,46 @@
     return gated_rows
 
 
-splits = ((64, 16), (64, 16))
+chunks = 2
+alone = 16
 halves = 2
+kinds = 18
+(
+    FORWARD, KEYS, PASS, ACTIVATE, FINISH, HOME, MEMORY, DOWN, OWN_KEYS,
+    SHARED, SHARED_DOWN, TEAM, TEAM_DONE, PROJECT, PAIR, PROJECTED, SHARED_TEAM, LAST,
+) = range(kinds)
+PLANS = {
+    4: (
+        (
+            224, 256, 97, 8, 288, 65, 9, 352, 104, 72, 16, 384, 73, 136, 128, 17,
+            129, 64, 108, 80, 24, 81, 116, 25, 112, 192, 88, 416, 120, 148, 149, 89,
+            140, 141, 137, 100, 144, 145, 176, 177, 124, 152, 168, 448, 169, 156, 153, 157,
+            320, 184, 132, 133, 185, 512, 544, 545, 480,
+        ),
+        (
+            224, 16, 0, 288, 105, 17, 112, 80, 1, 352, 384, 96, 136, 24, 73, 81,
+            25, 128, 137, 256, 144, 64, 32, 65, 145, 116, 88, 100, 89, 72, 148, 149,
+            120, 132, 133, 124, 108, 176, 192, 320, 200, 416, 156, 157, 152, 160, 140, 129,
+            448, 184, 161, 512, 141, 177, 153, 185, 544, 545, 480,
+        ),
+        (
+            224, 24, 80, 8, 113, 9, 25, 81, 120, 352, 384, 104, 0, 72, 73, 88,
+            1, 96, 89, 136, 108, 40, 124, 152, 153, 32, 64, 288, 140, 65, 137, 116,
+            256, 141, 156, 157, 100, 128, 129, 168, 320, 208, 200, 169, 192, 132, 133, 184,
+            416, 448, 185, 148, 160, 512, 149, 161, 144, 145, 544, 480, 545,
+        ),
+        (
+            224, 121, 16, 288, 17, 112, 256, 88, 80, 8, 81, 9, 352, 72, 116, 0,
+            73, 104, 384, 144, 148, 108, 1, 96, 145, 136, 40, 89, 152, 176, 140, 141,
+            32, 64, 65, 153, 124, 128, 100, 48, 149, 168, 200, 137, 320, 169, 216, 192,
+            132, 133, 208, 416, 177, 448, 160, 156, 157, 129, 161, 512, 544, 545, 480,
+        ),
+    ),
+}
 
 
 def lane_kernel(
-    lines,
+    lines, plan,
     ig_ref, fg_ref, gain_ref, ids_ref, rw_ref,
     q_ref, k_ref, v_ref, og_ref, mw_ref, x_ref, g_ref, u_ref, d_ref, sg_ref, su_ref, sd_ref,
     mo_ref, eo_ref,
@@ -165,31 +199,19 @@
     greet(me, other_y)
     greet(me, buddy)
 
-    bounds = []
-    at = 0
-    for size, only in splits:
-        bounds.append((at, size, only))
-        at += size
+    chunk = rows // chunks
 
     def z_copy(zb, way, n):
-        start, size, _ = bounds[n]
-        ref = tok.at[zb * 2 + x, start : start + size]
+        ref = tok.at[zb * 2 + x, sublanes(n * chunk, chunk)]
         to = z + 1 - 2 * way
         return remote(ref, ref, z_send.at[way, zb, n], z_recv.at[zb, n], to * 2 + x, j)
 
     def x_copy(zb, column, n):
-        start, size, only = bounds[n]
-        ref = tok.at[zb * 2 + column, sublanes(start + y * only, size - only)]
+        ref = tok.at[zb * 2 + column, sublanes(n * chunk + y * alone, chunk - alone)]
         return remote(ref, ref, x_send.at[zb, n], x_recv.at[zb, n], across, j)
 
-    def x_arrival(zb, n):
-        start, size, only = bounds[n]
-        ref = tok.at[zb * 2 + 1 - x, sublanes(start + y * only, size - only)]
-        return remote(ref, ref, x_send.at[zb, n], x_recv.at[zb, n], across, j)
-
     def e_copy(zb, n):
-        start, size, only = bounds[n]
-        ref = tok.at[zb * 2 + 1 - x, sublanes(start + y * (size - only), only)]
+        ref = tok.at[zb * 2 + 1 - x, sublanes(n * chunk + y * (chunk - alone), alone)]
         return remote(ref, ref, e_send.at[zb, n], e_recv.at[zb, n], me, other_y)
 
     def kz_copy(zb):
@@ -242,21 +264,21 @@
         return remote(refs[n], refs[n], f_send.at[n], f_recv.at[n], me, buddy)
 
     def xo_copy(zb, n):
-        cols = pl.ds(n * piece, piece)
+        cols = lanes(n * piece, piece)
         return remote(
             res.at[zb * 2 + 1 - x, :, cols], xin.at[zb, :, cols],
             xo_send.at[zb, n], xo_recv.at[zb, n], across, j,
         )
 
     def zo_copy(zb, n):
-        cols = pl.ds(n * piece, piece)
+        cols = lanes(n * piece, piece)
         return remote(
             zout.at[zb, :, cols], zin.at[z, :, cols],
             zo_send.at[zb, n], zo_recv.at[z, n], zb * 2 + x, j,
         )
 
     def zo_arrival(zb, n):
-        cols = pl.ds(n * piece, piece)
+        cols = lanes(n * piece, piece)
         return remote(
             zout.at[zb, :, cols], zin.at[zb, :, cols],
             zo_send.at[zb, n], zo_recv.at[zb, n], zb * 2 + x, j,
@@ -306,26 +328,26 @@
         jnp.sum(kept, axis=1, keepdims=True), (1, length)
     )
 
-    def normalize(start, size):
-        def group(n, carry):
-            at_rows = sublanes(start + n * 16, 16)
+    def normalize(n):
+        def group(i, carry):
+            at_rows = sublanes(n * chunk + i * 16, 16)
             wide_rows = xbuf[at_rows, :].astype(wide)
             scale = lax.rsqrt(jnp.mean(wide_rows * wide_rows, axis=1, keepdims=True) + epsilon)
             tok[me, at_rows, :] = (wide_rows * scale * gain_ref[...]).astype(low)
             return carry
 
-        lax.fori_loop(0, size // 16, group, 0)
+        lax.fori_loop(0, chunk // 16, group, 0)
 
     def can_go(way):
         to = z + 1 - 2 * way
         return (to >= 0) & (to < lines)
 
     load(0).wait()
-    normalize(bounds[0][0], bounds[0][1])
+    normalize(0)
     pl.semaphore_wait(barrier, ep_count + 1)
-    for n in range(len(bounds)):
+    for n in range(chunks):
         if n:
-            normalize(bounds[n][0], bounds[n][1])
+            normalize(n)
         for way in range(2):
 
             @pl.when(can_go(way))
@@ -336,121 +358,104 @@
         if n == 0:
             for i in range(6):
                 b_copy(c, i).start()
-            y_copy(y, 0).start()
     for k in range(1, ep_count):
         s_copy(k).start()
-    load(3).wait()
-    load(4).wait()
-
-    @pl.when(z + 1 < lines)
-    def _():
-        kz_copy(z).start()
-
-    @pl.when(x == 0)
-    def _():
-        kx_copy(z, x).start()
-
-    load(1).wait()
-    load(2).wait()
-    b_copy(1 - c, 0).wait_recv()
-    b_copy(1 - c, 1).wait_recv()
-
-    def activate(block):
+
+    def forward(zb, n):
+        way = jnp.where(zb < z, 0, 1)
+        z_copy(zb, way, n).wait_recv()
+
+        @pl.when(can_go(way))
+        def _():
+            z_copy(zb, way, n).start()
+
+        x_copy(zb, x, n).start()
+
+    def keys(zb):
+        kz_copy(zb).wait_recv()
+
+        @pl.when(z + 1 < lines)
+        def _():
+            kz_copy(zb).start()
+
+        kx_copy(zb, x).start()
+
+    def own_keys():
+        load(3).wait()
+        load(4).wait()
+
+        @pl.when(z + 1 < lines)
+        def _():
+            kz_copy(z).start()
+
+        @pl.when(x == 0)
+        def _():
+            kx_copy(z, x).start()
+
+    def pass_on(zb, n):
+        x_copy(zb, 1 - x, n).wait_recv()
+        e_copy(zb, n).start()
+
+    def gated_product(rows_in, gate_weight, up_weight):
+        gate = jnp.dot(rows_in, gate_weight, preferred_element_type=wide)
+        up = jnp.dot(rows_in, up_weight, preferred_element_type=wide)
+        return (gate / (1.0 + jnp.exp(-gate)) * up).astype(low)
+
+    def activate(zb, far, first):
+        @pl.when(first == 1)
+        def _():
+            for n in (1, 2):
+                load(n).wait()
+                b_copy(1 - c, n - 1).wait_recv()
+
+        @pl.when(far == 1)
+        def _():
+            for n in range(chunks):
+                e_copy(zb, n).wait_recv()
+
+        block = zb * 2 + jnp.where(far == 1, 1 - x, x)
         for h in range(2):
-            gate = jnp.dot(tok[block], gall[h], preferred_element_type=wide)
-            up = jnp.dot(tok[block], uall[h], preferred_element_type=wide)
-            act[block, y, :, h * units : (h + 1) * units] = (
-                gate / (1.0 + jnp.exp(-gate)) * up
-            ).astype(low)
+            act[block, y, :, h * units : (h + 1) * units] = gated_product(
+                tok[block], gall[h], uall[h]
+            )
         a_copy(block, y).start()
 
-    def valid(s, d, zb):
-        return (s >= 0) & (s < lines) & (zb >= 0) & (zb < lines) & ((s > 0) | (d == 0))
-
-    def both_ways(s, work):
-        def one(d, carry):
-            zb = z + s * (2 * d - 1)
-
-            @pl.when(valid(s, d, zb))
-            def _():
-                work(d, zb)
-
-            return carry
-
-        lax.fori_loop(0, 2, one, 0)
-
-    def forward(d, zb):
-        for n in range(len(bounds)):
-            z_copy(zb, d, n).wait_recv()
-
-            @pl.when(can_go(d))
-            def _():
-                z_copy(zb, d, n).start()
-
-            x_copy(zb, x, n).start()
-
-        @pl.when(d == 0)
-        def _():
-            kz_copy(zb).wait_recv()
-
-            @pl.when(z + 1 < lines)
-            def _():
-                kz_copy(zb).start()
-
-            kx_copy(zb, x).start()
-
-    def pass_on(d, zb):
-        for n in range(len(bounds)):
-            x_arrival(zb, n).wait_recv()
-            if bounds[n][2]:
-                e_copy(zb, n).start()
-
-    def near(d, zb):
-        activate(zb * 2 + x)
-
-    def far(d, zb):
-        for n in range(len(bounds)):
-            if bounds[n][2]:
-                e_copy(zb, n).wait_recv()
-        activate(zb * 2 + 1 - x)
-
-    def finish(block):
-        a_copy(block, 1 - y).wait_recv()
+    def finish(zb, far, n):
+        block = zb * 2 + jnp.where(far == 1, 1 - x, x)
+
+        @pl.when(n == 0)
+        def _():
+            a_copy(block, 1 - y).wait_recv()
+
         weight = jnp.sum(
             jnp.where(at_row == at_lane, side[block, pl.ds(me, 1), :], 0.0), axis=1, keepdims=True
         )
-        for n in range(halves):
-            cols = slice(n * piece, (n + 1) * piece)
-            total = jnp.dot(act[block, 0], dall[0, :, cols], preferred_element_type=wide)
-            total += jnp.dot(act[block, 1], dall[1, :, cols], preferred_element_type=wide)
-            res[block, :, cols] = (total * weight).astype(low)
-
-    def finish_near(d, zb):
-        finish(zb * 2 + x)
-
-    def finish_far(d, zb):
-        finish(zb * 2 + 1 - x)
-        for n in range(halves):
+        cols = lanes(n * piece, piece)
+        total = jnp.dot(act[block, 0], dall[0, :, cols], preferred_element_type=wide)
+        total += jnp.dot(act[block, 1], dall[1, :, cols], preferred_element_type=wide)
+        res[block, :, cols] = (total * weight).astype(low)
+
+        @pl.when(far == 1)
+        def _():
             xo_copy(zb, n).start()
 
-    def send_home(d, zb):
-        for n in range(halves):
-            cols = slice(n * piece, (n + 1) * piece)
-            xo_copy(zb, n).wait_recv()
-            zout[zb, :, cols] = (
-                res[zb * 2 + x, :, cols].astype(wide) + xin[zb, :, cols].astype(wide)
-            ).astype(low)
-            zo_copy(zb, n).start()
-
-    def memory(d, zb):
-        @pl.when((d == 0) & (zb * 2 + 1 - x < me))
+    def send_home(zb, n):
+        cols = lanes(n * piece, piece)
+        xo_copy(zb, n).wait_recv()
+        zout[zb, :, cols] = (
+            res[zb * 2 + x, :, cols].astype(wide) + xin[zb, :, cols].astype(wide)
+        ).astype(low)
+        zo_copy(zb, n).start()
+
+    def memory(zb):
+        @pl.when(zb * 2 + 1 - x < me)
         def _():
             kx_copy(zb, 1 - x).wait_recv()
 
         def one(n, carry):
             block = zb * 2 + n
 
-            @pl.when((d == 0) & (block <= me))
+            @pl.when(block <= me)
             def _():
                 scores = lax.dot_general(
                     qb[...], kvb[block, :, :key_dim], (((1,), (1,)), ((), ())),
@@ -470,7 +475,19 @@
 
         lax.fori_loop(0, 2, one, 0)
 
-    def prepare():
+    def shared_hidden():
+        for n in (2, 3):
+            load(n + 6).wait()
+            b_copy(1 - c, n).wait_recv()
+        for h in range(2):
+            sall[y, :, h * shared : (h + 1) * shared] = gated_product(
+                tok[me], sgall[h], suall[h]
+            )
+        y_copy(y, 2).start()
+
+    def team():
+        y_copy(1 - y, 0).wait_recv()
+        f_copy(c, 0).start()
         for k in range(1, ep_count):
             s_arrival(k).wait_recv()
         gap = jnp.zeros((1, length), wide)
@@ -482,93 +499,56 @@
             brow[b, 0:1, :] = row
             top = jnp.where(earlier, jnp.maximum(top, row), top)
         own = side[me, ep_count : ep_count + 1, :]
-        within = jnp.max(
-            jnp.where(at_row >= at_lane, own, lowest), axis=1, keepdims=True
-        )
+        within = jnp.max(jnp.where(at_row >= at_lane, own, lowest), axis=1, keepdims=True)
         before = jnp.max(jnp.maximum(top, gap), axis=1, keepdims=True)
         stab[...] = jnp.broadcast_to(jnp.maximum(within, before), stab.shape)
         num[...] = jnp.zeros_like(num)
         den[...] = jnp.zeros_like(den)
         load(6).wait()
-        load(8).wait()
-        load(9).wait()
-        for n in (2, 3):
-            b_copy(1 - c, n).wait_recv()
-        for h in range(2):
-            gate = jnp.dot(tok[me], sgall[h], preferred_element_type=wide)
-            up = jnp.dot(tok[me], suall[h], preferred_element_type=wide)
-            sall[y, :, h * shared : (h + 1) * shared] = (
-                gate / (1.0 + jnp.exp(-gate)) * up
-            ).astype(low)
-        for n in (1, 2):
-            y_copy(y, n).start()
         load(5).wait()
-        y_copy(1 - y, 0).wait_recv()
-        f_copy(c, 0).start()
         b_copy(1 - c, 4).wait_recv()
-        f_copy(1 - c, 0).wait_recv()
-
-    def step(t, carry):
-        both_ways(jnp.where(t > 0, t, lines), forward)
-        both_ways(jnp.where(t > 2, t - 2, lines), finish_far)
-        both_ways(t - 1, pass_on)
-        both_ways(t, near)
-        both_ways(jnp.where(t > 3, t - 3, lines), send_home)
-        both_ways(t - 1, far)
-
-        @pl.when(t == 1)
-        def _():
-            prepare()
-
-        both_ways(t - 1, memory)
-        both_ways(t - 1, finish_near)
-        return carry
-
-    lax.fori_loop(0, lines + 1, step, 0)
-
-    def late(n, carry):
-        both_ways(jnp.where(n == 0, lines - 1, 0), finish_far)
-
+
+    def project():
+        load(7).wait()
+        load(11).wait()
+        hidden = num[...] / jnp.maximum(jnp.abs(den[:, 0:1]), den_floor)
+        gated = (hidden * (1.0 / (1.0 + jnp.exp(-ogb[...].astype(wide))))).astype(low)
+        for n in range(4):
+            cols = slice(n * half // 2, (n + 1) * half // 2)
+            mpart[:, cols] = jnp.dot(gated, mwb[:, cols], preferred_element_type=wide).astype(low)
+        m_copy(c, 0).start()
+
+    def pair():
+        m_copy(c, 0).wait_recv()
+        msum[...] = (
+            mpart[sublanes(c * part, part), :].astype(wide) + mpeer[...].astype(wide)
+        ).astype(low)
+        m_copy(c, 1).start()
+
+    def projected():
+        m_copy(c, 1).wait_recv()
+        mo_ref[sublanes(c * part, part), :] = (
+            msum[...].astype(wide) + mother[...].astype(wide)
+        ).astype(low)
+        m_copy(c, 2).start()
+
+    def shared_team():
+        y_copy(1 - y, 1).wait_recv()
+        f_copy(c, 1).start()
+        y_copy(1 - y, 2).wait_recv()
+        load(10).wait()
+        b_copy(1 - c, 5).wait_recv()
+
+    def last(n):
         @pl.when(n == 0)
         def _():
-            both_ways(lines - 2, send_home)
-
-        return carry
-
-    lax.fori_loop(0, 2, late, 0)
-
-    load(7).wait()
-    load(11).wait()
-    hidden = num[...] / jnp.maximum(jnp.abs(den[:, 0:1]), den_floor)
-    gated = (hidden * (1.0 / (1.0 + jnp.exp(-ogb[...].astype(wide))))).astype(low)
-    for n in range(4):
-        cols = slice(n * half // 2, (n + 1) * half // 2)
-        mpart[:, cols] = jnp.dot(gated, mwb[:, cols], preferred_element_type=wide).astype(low)
-    m_copy(c, 0).start()
-    load(10).wait()
-    y_copy(1 - y, 1).wait_recv()
-    f_copy(c, 1).start()
-    y_copy(1 - y, 2).wait_recv()
-    b_copy(1 - c, 5).wait_recv()
-    m_copy(c, 0).wait_recv()
-    msum[...] = (
-        mpart[sublanes(c * part, part), :].astype(wide) + mpeer[...].astype(wide)
-    ).astype(low)
-    m_copy(c, 1).start()
-    both_ways(lines - 1, send_home)
-    f_copy(1 - c, 1).wait_recv()
-    m_copy(c, 1).wait_recv()
-    mo_ref[sublanes(c * part, part), :] = (
-        msum[...].astype(wide) + mother[...].astype(wide)
-    ).astype(low)
-    m_copy(c, 2).start()
-
-    for n in range(halves):
-        cols = slice(n * piece, (n + 1) * piece)
+            f_copy(1 - c, 1).wait_recv()
+
+        cols = lanes(n * piece, piece)
         xo_copy(z, n).wait_recv()
         total = res[me, :, cols].astype(wide) + xin[z, :, cols].astype(wide)
-        for team in range(2):
-            total += jnp.dot(sall[team], sdall[team, :, cols], preferred_element_type=wide)
+        for k in range(2):
+            total += jnp.dot(sall[k], sdall[k, :, cols], preferred_element_type=wide)
         for k in range(1, lines):
             source = lax.rem(z + k, lines)
             zo_arrival(source, n).wait_recv()
@@ -576,6 +556,57 @@
         eo_ref[sublanes(c * rows, rows), lanes(y * half + n * piece, piece)] = total.astype(low)
         ey_copy(y, n).start()
         eb_copy(c, n).start()
+
+    events = {
+        FORWARD: lambda zb, far, n: forward(zb, n),
+        KEYS: lambda zb, far, n: keys(zb),
+        PASS: lambda zb, far, n: pass_on(zb, n),
+        ACTIVATE: activate,
+        FINISH: finish,
+        HOME: lambda zb, far, n: send_home(zb, n),
+        MEMORY: lambda zb, far, n: memory(zb),
+        DOWN: lambda zb, far, n: y_copy(y, 0).start(),
+        OWN_KEYS: lambda zb, far, n: own_keys(),
+        SHARED: lambda zb, far, n: shared_hidden(),
+        SHARED_DOWN: lambda zb, far, n: y_copy(y, 1).start(),
+        TEAM: lambda zb, far, n: team(),
+        TEAM_DONE: lambda zb, far, n: f_copy(1 - c, 0).wait_recv(),
+        PROJECT: lambda zb, far, n: project(),
+        PAIR: lambda zb, far, n: pair(),
+        PROJECTED: lambda zb, far, n: projected(),
+        SHARED_TEAM: lambda zb, far, n: shared_team(),
+        LAST: lambda zb, far, n: last(n),
+    }
+    longest = max(len(order) for order in plan)
+    words = []
+    for at in range(0, longest, 3):
+        word = jnp.int32(0)
+        for k, order in enumerate(plan):
+            packed = 0
+            for code in reversed((order + (1023,) * longest)[at : at + 3]):
+                packed = packed * 1024 + code
+            word = jnp.where(z == k, packed, word)
+        words.append(word)
+
+    def event(i, carry):
+        at, place = lax.div(i, 3), lax.rem(i, 3)
+        word = words[0]
+        for k in range(1, len(words)):
+            word = jnp.where(at == k, words[k], word)
+        code = jnp.where(place == 0, word, jnp.where(place == 1, word // 1024, word // 1048576))
+        code = lax.rem(code, 1024)
+        kind, arg = lax.div(code, 8 * lines), lax.rem(code, 8 * lines)
+        zb, far, n = lax.div(arg, 8), lax.rem(lax.div(arg, 4), 2), lax.rem(arg, 4)
+        for k, work in events.items():
+
+            @pl.when(kind == k)
+            def _():
+                work(zb, far, n)
+
+        return carry
+
+    lax.fori_loop(0, longest, event, 0)
+
     for n in range(halves):
         ey_copy(1 - y, n).wait_recv()
         ef_copy(c, n).start()
@@ -608,7 +639,7 @@
 
             @pl.when(can_go(way) & passing)
             def _():
-                for n in range(len(bounds)):
+                for n in range(chunks):
                     z_copy(zb, way, n).wait_send()
 
         @pl.when((z + 1 < lines) & (zb <= z))
@@ -619,10 +650,9 @@
         def _():
             kx_copy(zb, x).wait_send()
 
-        for n in range(len(bounds)):
+        for n in range(chunks):
             x_copy(zb, x, n).wait_send()
-            if bounds[n][2]:
-                e_copy(zb, n).wait_send()
+            e_copy(zb, n).wait_send()
         for n in range(halves):
             xo_copy(zb, n).wait_send()
 
@@ -650,7 +680,6 @@
     units, shared = expert_gate.shape[2], shared_gate.shape[1]
     low, wide, dma = jnp.bfloat16, jnp.float32, pltpu.SemaphoreType.DMA
     side_rows = ep_count + 2 + -(ep_count + 2) % 8
-    chunks = len(splits)
     vmem = pl.BlockSpec(memory_space=pltpu.VMEM)
     hbm = pl.BlockSpec(memory_space=pl.ANY)
 
@@ -658,7 +687,7 @@
         return pltpu.VMEM(shape, dtype)
 
     return pl.pallas_call(
-        functools.partial(lane_kernel, lines),
+        functools.partial(lane_kernel, lines, PLANS[lines]),
         out_shape=(
             jax.ShapeDtypeStruct((length, width), low),
             jax.ShapeDtypeStruct((tokens, width), low),
@@ -809,7 +838,7 @@
     tokens, slots = expert_input.shape[0], route_ids.shape[1] * 2 * expert_input.shape[0]
     per_ep = tp_count * expert_gate.shape[2] // FF
     even = ep_count % 2 == 0 and tp_count == 4 and MEMORY_HEADS * 2 == tp_count
-    blocked = values.shape[0] == BLOCK and tokens == 2 * BLOCK and ep_count > 2
+    blocked = values.shape[0] == BLOCK and tokens == 2 * BLOCK and ep_count // 2 in PLANS
     dense = even and blocked and per_ep == 1 and slots // (ep_count * per_ep) >= tokens
     experts = (
         expert_input,

time: 101 us -> 89.5 us (0.89)
  Pallas kernels: 97.1 us -> 85.7 us
    pallas_call x1, Pallas kernels: 97.1 us -> 85.7 us  [lane_program(): pl.pallas_call(functools.partial(lane_kernel, lines, PLANS[lines]), out_s...]
where the time goes in v2:
time: 89.5 us; the launch traced here: 89.3 us
  Pallas kernels  85.7 us (96%)
  local copies, waits for them, and re-layouts  2.94 us (3%)
    pallas_call x1, Pallas kernels, lane_program(): pl.pallas_call(functools.partial(lane_kernel, lines, PLANS[lines]), out_s...  85.7 us
    unnamed x4, local copies, waits for them, and re-layouts  2.94 us

profile of v2, /device:TPU:0, one launch (start us, length us, event | category | flops | bytes accessed | tf_op | source)
XLA Modules:
  0.0 89.3 jit_solution(3874982870842737905)
XLA Ops:
  0.6 85.7 %shard_map.176 = (bf16[128,2048]{1,0:T(8,128)(2,1)}, bf16[256,2048]{1,0:T(8,128)(2,1)}) custom-call(f32[2,128]{1,0:T(2,128)} %bitcast.8, f32[2,128]{1,0:T(2,128)} %bitcast.9, f32[1,2048]{1,0:T(1,128)} %bitcast.5, s32[4,256]{1,0:T(4,128)} %bitcast.6, f32[4,256]{1,0:T(4,128)} %bitcast.7, bf16[128,512]{1,0:T(8,128)(2,1)} %q_ref.1, bf16[128,512]{1,0:T(8,128)(2,1)} %k_ref.1, ...), custom_call_target="tpu_custom_call" | custom-call | tf_op jit(solution)/shard_map/pallas_call | solution.py:689
  86.3 0.0 copy-start
  86.3 2.0 %copy.21 = bf16[128,2048]{1,0:T(8,128)(2,1)} copy(bf16[128,2048]{1,0:T(8,128)(2,1)} %get-tuple-element.4) | data formatting | bytes 1048576
  88.3 0.0 copy-done
  88.3 1.0 %copy.22 = bf16[256,2048]{1,0:T(8,128)(2,1)} copy(bf16[256,2048]{1,0:T(8,128)(2,1)S(1)} %copy-done) | data formatting | bytes 2097152
Async XLA Ops:
  86.3 2.0 %copy-start = (bf16[256,2048]{1,0:T(8,128)(2,1)S(1)}, bf16[256,2048]{1,0:T(8,128)(2,1)}, u32[]{:S(2)}) copy-start(bf16[256,2048]{1,0:T(8,128)(2,1)} %get-tuple-element.5) | copy-start | bytes 3145732

commit v3 on v2

--- a/solution.py
+++ b/solution.py
@@ -597,11 +597,24 @@
         code = lax.rem(code, 1024)
         kind, arg = lax.div(code, 8 * lines), lax.rem(code, 8 * lines)
         zb, far, n = lax.div(arg, 8), lax.rem(lax.div(arg, 4), 2), lax.rem(arg, 4)
-        for k, work in events.items():
-
-            @pl.when(kind == k)
+
+        def choose(low_kind, high_kind):
+            if high_kind - low_kind == 1:
+                events[low_kind](zb, far, n)
+                return
+            middle = (low_kind + high_kind) // 2
+
+            @pl.when(kind < middle)
             def _():
-                work(zb, far, n)
+                choose(low_kind, middle)
+
+            @pl.when(kind >= middle)
+            def _():
+                choose(middle, high_kind)
+
+        @pl.when(kind < kinds)
+        def _():
+            choose(0, kinds)
 
         return carry
 
@@ -665,6 +678,17 @@
         return carry
 
     lax.fori_loop(0, lines, drain, 0)
+
+
+def write_kernel(mixed_ref, routed_ref, mo_ref, eo_ref, sem):
+    copies = [
+        pltpu.make_async_copy(routed_ref, eo_ref, sem.at[0]),
+        pltpu.make_async_copy(mixed_ref, mo_ref, sem.at[1]),
+    ]
+    for copy in copies:
+        copy.start()
+    for copy in copies:
+        copy.wait()
 
 
 def lane_program(
@@ -686,13 +710,13 @@
     def buffer(*shape, dtype=low):
         return pltpu.VMEM(shape, dtype)
 
-    return pl.pallas_call(
+    results = pl.pallas_call(
         functools.partial(lane_kernel, lines, PLANS[lines]),
         out_shape=(
             jax.ShapeDtypeStruct((length, width), low),
             jax.ShapeDtypeStruct((tokens, width), low),
         ),
-        in_specs=[vmem] * 5 + [hbm] * 12,
+        in_specs=[vmem] * 5 + [pl.BlockSpec(memory_space=pltpu.HBM)] * 12,
         out_specs=(vmem, vmem),
         scratch_shapes=[
             buffer(rows, width),
@@ -737,13 +761,34 @@
             dma((3,)), dma((3,)),
         ],
         compiler_params=pltpu.CompilerParams(
-            collective_id=0, has_side_effects=True, vmem_limit_bytes=56 * 1024 * 1024
+            collective_id=0, has_side_effects=True, vmem_limit_bytes=40 * 1024 * 1024
         ),
     )(
-        input_gate.T, forget_gate.T, norm_gain[None, :], route_ids.T, route_weights.T,
-        queries, key_vectors, values, out_gate, mix_weight, expert_input,
-        expert_gate, expert_up, expert_down, shared_gate, shared_up, shared_down,
-    )
+        *(
+            pltpu.with_memory_space_constraint(array, pltpu.HBM)
+            for array in (
+                input_gate.T, forget_gate.T, norm_gain[None, :], route_ids.T, route_weights.T,
+            )
+        ),
+        *(
+            pltpu.with_memory_space_constraint(array, pltpu.HBM)
+            for array in (
+                queries, key_vectors, values, out_gate, mix_weight, expert_input,
+                expert_gate, expert_up, expert_down, shared_gate, shared_up, shared_down,
+            )
+        ),
+    )
+    return pl.pallas_call(
+        write_kernel,
+        out_shape=(
+            jax.ShapeDtypeStruct((length, width), low),
+            jax.ShapeDtypeStruct((tokens, width), low),
+        ),
+        in_specs=[hbm, hbm],
+        out_specs=(hbm, hbm),
+        scratch_shapes=[dma((2,))],
+        compiler_params=pltpu.CompilerParams(vmem_limit_bytes=1024 * 1024),
+    )(*results)
 
 
 def expert_half(

time: 89.5 us -> 86.5 us (0.966)
  local copies, waits for them, and re-layouts: 2.94 us -> 0 us
    unnamed x4 -> x0, local copies, waits for them, and re-layouts: 2.94 us -> none
    pallas_call x1, Pallas kernels: 85.7 us -> 84.5 us  [lane_program(): pl.pallas_call(functools.partial(lane_kernel, lines, PLANS[lines]), out_s...]
    pallas_call x0 -> x1, Pallas kernels: none -> 1.16 us  [lane_program(): pl.pallas_call(write_kernel, out_shape=(jax.ShapeDtypeStruct((length, wid...]
where the time goes in v3:
time: 86.5 us; the launch traced here: 86.3 us
  Pallas kernels  85.6 us (99%)
    pallas_call x1, Pallas kernels, lane_program(): pl.pallas_call(functools.partial(lane_kernel, lines, PLANS[lines]), out_s...  84.5 us

profile of v3, /device:TPU:0, one launch (start us, length us, event | category | flops | bytes accessed | tf_op | source)
XLA Modules:
  0.0 86.3 jit_solution(3043397372566414024)
XLA Ops:
  0.6 84.5 %shard_map.176 = (bf16[128,2048]{1,0:T(8,128)(2,1)S(1)}, bf16[256,2048]{1,0:T(8,128)(2,1)S(1)}) custom-call(f32[2,128]{1,0:T(2,128)} %bitcast.8, f32[2,128]{1,0:T(2,128)} %bitcast.9, f32[1,2048]{1,0:T(1,128)} %bitcast.5, s32[4,256]{1,0:T(4,128)} %bitcast.6, f32[4,256]{1,0:T(4,128)} %bitcast.7, bf16[128,512]{1,0:T(8,128)(2,1)} %q_ref.1, ...), custom_call_target="tpu_custom_call" | custom-call | tf_op jit(solution)/shard_map/pallas_call | solution.py:713
  85.1 1.2 %shard_map.177 = (bf16[128,2048]{1,0:T(8,128)(2,1)}, bf16[256,2048]{1,0:T(8,128)(2,1)}) custom-call(bf16[128,2048]{1,0:T(8,128)(2,1)S(1)} %get-tuple-element.4.mixed_ref, bf16[256,2048]{1,0:T(8,128)(2,1)S(1)} %get-tuple-element.5.routed_ref), custom_call_target="tpu_custom_call" | custom-call | tf_op jit(solution)/shard_map/pallas_call | solution.py:781
